TPU v7x, 256 devices: a whole 4x4x8 slice. The times are simulated.
256 devices in a mesh: ep: 16 (over y, x), tp: 16 (over z, core).
Axes of the slice: x: 4, y: 4, z: 8, core: 2. Of those that a mesh axis runs over, the one named last changes fastest.
Arguments:
- tokens: bfloat16 [1024, 2048], P('ep'), may hold values from -7 to 7
- state: float32 [1024, 32, 64, 64], P('ep', 'tp'), may hold values from -6 to 6
- routes: int32 [1024, 2], P('ep'), may hold values from 0 to 15, all different within a row; in each aligned block of 64 rows (0 to 63, 64 to 127, ...) at most 12 rows name the same one
- route_logits: float32 [1024, 2], P('ep'), may hold values from -4 to 4
- mix_gain: float32 [2048], replicated, may hold values from 0.1 to 1.9
- w_recept: bfloat16 [2048, 2048], P(None, 'tp')
- w_key: bfloat16 [2048, 2048], P(None, 'tp'), may hold values from -0.125 to 0.125
- w_value: bfloat16 [2048, 2048], P(None, 'tp'), may hold values from -0.125 to 0.125
- w_decay: bfloat16 [2048, 2048], P(None, 'tp'), may hold values from -0.125 to 0.125
- w_rate: bfloat16 [2048, 2048], P(None, 'tp'), may hold values from -0.125 to 0.125
- decay_base: float32 [2048], P('tp'), may hold values from -3 to 1
- rate_base: float32 [2048], P('tp'), may hold values from -3 to 3
- key_gain: float32 [2048], P('tp'), may hold values from 0.1 to 1.9
- group_gain: float32 [2048], P('tp'), may hold values from 0.1 to 1.9
- w_output: bfloat16 [2048, 2048], P('tp'), may hold values from -0.125 to 0.125
- ffn_gain: float32 [2048], replicated, may hold values from 0.1 to 1.9
- w_gate: bfloat16 [16, 2048, 7168], P('ep', None, 'tp'), may hold values from -0.125 to 0.125
- w_up: bfloat16 [16, 2048, 7168], P('ep', None, 'tp'), may hold values from -0.125 to 0.125
- w_down: bfloat16 [16, 7168, 2048], P('ep', 'tp'), may hold values from -0.0625 to 0.0625
Outputs:
- output: bfloat16 [1024, 2048], P('ep', 'tp')
- new_state: float32 [1024, 32, 64, 64], P('ep', 'tp')
Inputs may be any that keep to these rules, and one draw needn't show every extreme that they name: `routes`: for each expert, the 64 tokens of one device group's rows name it in at most 12 of their rows; the 2 experts of a row differ.
All inputs are finite; a program needn't handle non-finite values.
Results may differ from a plain program's by a relative error of at most 0.0091.
Values may be sent and summed in bfloat16 or wider, within the bound.
A program may use at most 64 MiB of HBM per device.

v0:
```python
import jax
import jax.numpy as jnp
from jax import lax
from jax.sharding import Mesh
from jax.sharding import PartitionSpec as P

TP = ("tp_0", "tp_1")


RMS_EPS = 1e-06
GROUP_EPS = 0.00064
UNIT_EPS = 6.4e-05
HIGHEST = lax.Precision.HIGHEST


def cut_along(shard, dim, devices):
    before, after = (shard.shape[:dim], shard.shape[dim + 1 :])
    return jnp.moveaxis(shard.reshape(*before, devices, -1, *after), dim, 0)


def sum_at_owner(shard, axis, dim):
    pieces = cut_along(shard, dim, lax.axis_size(axis))
    arrived = lax.all_to_all(pieces, axis, split_axis=0, concat_axis=0, tiled=True)
    return arrived.astype(jnp.float32).sum(axis=0)


def from_everyone(shard, axis):
    copies = jnp.broadcast_to(shard, (lax.axis_size(axis), *shard.shape))
    return lax.all_to_all(copies, axis, split_axis=0, concat_axis=0, tiled=True)


def of_everyone(shard, axis):
    everything = from_everyone(shard, axis)
    return jnp.sum(everything, axis=0)


def gather_axes(shard, axes, dim):
    for axis in reversed(axes):
        shard = lax.all_gather(shard, axis, axis=dim, tiled=True)
    return shard


def rounded(values):
    return lax.optimization_barrier(values.astype(jnp.bfloat16)).astype(jnp.float32)


def mix_heads(
    normed,
    state,
    w_recept,
    w_key,
    w_value,
    w_decay,
    w_rate,
    decay_base,
    rate_base,
    key_gain,
    group_gain,
):
    seq_rows = state.shape[0]
    head_count = state.shape[1]

    def project(weight):
        return rounded(jnp.dot(normed, weight, preferred_element_type=jnp.float32))

    def split_heads(values):
        return values.reshape(seq_rows, head_count, -1)

    recept = split_heads(project(w_recept))
    keys_now = split_heads(project(w_key))
    values_now = split_heads(project(w_value))
    decay_pre = project(w_decay) + decay_base
    decay_now = split_heads(jnp.exp(-jnp.exp(-jax.nn.softplus(-decay_pre) - 0.5)))
    rate_now = split_heads(jax.nn.sigmoid(project(w_rate) + rate_base))
    scaled = keys_now * key_gain.reshape(head_count, -1)[None]
    unit_key = scaled * lax.rsqrt(jnp.sum(scaled * scaled, axis=2, keepdims=True) + UNIT_EPS)
    removed = jnp.einsum("bhvk,bhk->bhv", state, unit_key, precision=HIGHEST)
    new_state = (
        state * decay_now[:, :, None, :]
        - removed[:, :, :, None] * (unit_key * rate_now)[:, :, None, :]
        + values_now[:, :, :, None] * keys_now[:, :, None, :]
    )
    readout = jnp.einsum("bhvk,bhk->bhv", new_state, recept, precision=HIGHEST)
    centred = readout - jnp.mean(readout, axis=2, keepdims=True)
    spread = jnp.mean(centred * centred, axis=2, keepdims=True)
    normed_read = centred * lax.rsqrt(spread + GROUP_EPS) * group_gain.reshape(head_count, -1)[None]
    return (normed_read.reshape(seq_rows, -1).astype(jnp.bfloat16), new_state)


def slot_numbers(route_rows, expert_count, capacity):
    flat_routes = route_rows.reshape(-1)
    one_hot = (flat_routes[:, None] == jnp.arange(expert_count, dtype=jnp.int32)[None, :]).astype(
        jnp.int32
    )
    earlier = jnp.cumsum(one_hot, axis=0) - one_hot
    placed = jnp.sum(earlier * one_hot, axis=1)
    return (flat_routes * capacity + placed).reshape(route_rows.shape)


def local(
    tokens,
    state,
    routes,
    route_logits,
    mix_gain,
    w_recept,
    w_key,
    w_value,
    w_decay,
    w_rate,
    decay_base,
    rate_base,
    key_gain,
    group_gain,
    w_output,
    ffn_gain,
    w_gate,
    w_up,
    w_down,
):
    seq_rows, full_width = tokens.shape
    top_count = routes.shape[1]
    share_cols = full_width // lax.axis_size(TP)
    tp_index = lax.axis_index(TP)
    group_count = lax.axis_size("ep")
    capacity = max(2, 3 * top_count * seq_rows // (2 * group_count))
    slot_count = group_count * capacity
    values = tokens.astype(jnp.float32)
    normed = (
        values * lax.rsqrt(jnp.mean(values * values, axis=1, keepdims=True) + RMS_EPS) * mix_gain
    ).astype(jnp.bfloat16)
    mixed_rows, new_state = mix_heads(
        normed,
        state,
        w_recept,
        w_key,
        w_value,
        w_decay,
        w_rate,
        decay_base,
        rate_base,
        key_gain,
        group_gain,
    )
    partial_out = jnp.dot(mixed_rows, w_output, preferred_element_type=jnp.float32)
    slot_ids = slot_numbers(routes, group_count, capacity)
    slot_range = jnp.arange(slot_count, dtype=jnp.int32)
    pick_rows = jnp.any(slot_ids[None, :, :] == slot_range[:, None, None], axis=2).astype(
        jnp.bfloat16
    )
    route_exp = jnp.exp(route_logits)
    route_weight = route_exp / jnp.sum(route_exp, axis=1, keepdims=True)
    combine = jnp.sum(
        jnp.where(slot_ids[:, :, None] == slot_range[None, None, :], route_weight[:, :, None], 0.0),
        axis=1,
    )
    mix_part = sum_at_owner(partial_out.astype(jnp.bfloat16), TP, 1)
    own_vals = lax.dynamic_slice_in_dim(values, tp_index * share_cols, share_cols, 1)
    resid_own = (own_vals + mix_part).astype(jnp.bfloat16)
    resid_vals = resid_own.astype(jnp.float32)
    square_sum = of_everyone(jnp.sum(resid_vals * resid_vals, axis=1), TP)
    own_gain = lax.dynamic_slice_in_dim(ffn_gain, tp_index * share_cols, share_cols, 0)
    ffn_cols = (
        resid_vals * lax.rsqrt(square_sum / full_width + RMS_EPS)[:, None] * own_gain
    ).astype(jnp.bfloat16)
    outgoing = jnp.dot(pick_rows, ffn_cols, preferred_element_type=jnp.float32).astype(jnp.bfloat16)
    arrived = lax.all_to_all(
        outgoing.reshape(group_count, capacity, share_cols),
        "ep",
        split_axis=0,
        concat_axis=0,
        tiled=True,
    )
    slot_cols = arrived.reshape(slot_count, share_cols)
    gate_local = w_gate[0]
    up_local = w_up[0]
    segment = gather_axes(slot_cols, TP, 1)
    gate_act = jnp.dot(segment, gate_local, preferred_element_type=jnp.float32)
    upward = jnp.dot(segment, up_local, preferred_element_type=jnp.float32)
    hidden = (jax.nn.silu(gate_act) * upward).astype(jnp.bfloat16)
    expert_part = jnp.dot(hidden, w_down[0], preferred_element_type=jnp.float32)
    returned = lax.all_to_all(
        expert_part.reshape(group_count, capacity, full_width).astype(jnp.bfloat16),
        "ep",
        split_axis=0,
        concat_axis=0,
        tiled=True,
    ).astype(jnp.float32)
    moe_full = jnp.dot(
        combine,
        returned.reshape(slot_count, full_width),
        precision=HIGHEST,
        preferred_element_type=jnp.float32,
    )
    moe_own = sum_at_owner(moe_full.astype(jnp.bfloat16), TP, 1)
    output = (resid_own.astype(jnp.float32) + moe_own).astype(jnp.bfloat16)
    return (output, new_state)


def solution(mesh):
    torus = Mesh(mesh.devices.reshape(mesh.shape["ep"], 8, 2), ("ep", "tp_0", "tp_1"))
    return jax.shard_map(
        local,
        mesh=torus,
        in_specs=(
            P("ep", None),
            P("ep", TP, None, None),
            P("ep", None),
            P("ep", None),
            P(),
            P(None, TP),
            P(None, TP),
            P(None, TP),
            P(None, TP),
            P(None, TP),
            P(TP),
            P(TP),
            P(TP),
            P(TP),
            P(TP, None),
            P(),
            P("ep", None, TP),
            P("ep", None, TP),
            P("ep", TP, None),
        ),
        out_specs=(P("ep", TP), P("ep", TP, None, None)),
        check_vma=False,
    )
```

profile of v0, /device:TPU:1, one launch (start us, length us, event | category | flops | bytes accessed | tf_op | source)
XLA Modules:
  0.0 147.5 jit_solution(14206047786434785173)
XLA Ops:
  0.6 0.0 copy-start
  0.6 1.2 multiply_reduce_fusion
  1.9 1.4 convolution_convert_fusion.7
  3.3 0.1 reshape.117
  3.4 0.7 mul.173
  4.2 0.1 multiply_reduce_fusion.2
  4.3 1.4 convolution_convert_fusion.6
  5.8 0.7 add_divide_fusion
  6.4 0.1 reshape.109
  6.6 1.4 convolution_convert_fusion.8
  8.0 0.7 fusion.24
  8.7 0.1 mul.170
  8.8 1.4 convolution_convert_fusion.5
  10.2 0.1 reshape.118
  10.3 1.4 convolution_convert_fusion.4
  11.7 0.1 reshape.125
  11.8 0.0 copy-start.1
  11.8 0.1 fusion.28
  12.0 8.5 %fusion.29 = f32[64,2,1,64]{3,2,1,0:T(1,128)S(1)} fusion(f32[64,2,64,1]{2,3,1,0:T(1,128)S(1)} %bitcast.59, f32[64,2,64,64]{3,2,1,0:T(8,128)} %param.20), kind=kOutput, calls=%fused_computation.63 | convolution fusion | flops 6291456 | bytes 2162688 | tf_op jit(solution)/shard_map/bhvk,bhk->bhv/dot_general | solution.py:77
  20.4 2.7 %multiply_add_fusion = f32[64,2,64,64]{3,2,1,0:T(8,128)S(1)} fusion(f32[64,2,64,64]{3,2,1,0:T(8,128)S(1)} %copy-done.1, f32[64,2,64]{2,1,0:T(2,128)S(1)} %reshape.117, f32[64,2,64]{2,1,0:T(2,128)S(1)} %reshape.118, f32[64,2,64]{2,1,0:T(2,128)S(1)} %get-tuple-element.4, f32[64,2,64]{2,1,0:T(2,128)S(1)} %bitcast.58, f32[64,2,64]{2,1,0:T(2,128)S(1)} %mul.170), kind=kLoop, calls=%fused_computation | loop fusion | flops 2621440 | bytes 4358144 | tf_op jit(solution)/shard_map/add | solution.py:79
  23.2 0.0 copy-start.2
  23.2 2.0 %copy-done.2 = f32[64,2,64,64]{3,2,1,0:T(8,128)} copy-done((f32[64,2,64,64]{3,2,1,0:T(8,128)}, f32[64,2,64,64]{3,2,1,0:T(8,128)S(1)}, u32[]{:S(2)}) %copy-start.2) | copy-done | bytes 2097176
  25.2 3.4 %fusion.30 = f32[64,2,1,64]{3,2,1,0:T(1,128)S(1)} fusion(f32[64,2,64,64]{3,2,1,0:T(8,128)S(1)} %multiply_add_fusion, bf16[64,2,64,1]{2,3,1,0:T(2,128)(2,1)S(1)} %reshape.125), kind=kOutput, calls=%fused_computation.64 | convolution fusion | flops 6291456 | bytes 2146304 | tf_op jit(solution)/shard_map/bhvk,bhk->bhv/dot_general | solution.py:83
  28.6 0.1 reduce_sum.103
  28.8 0.2 multiply_reduce_fusion.1
  29.0 0.1 mul.191
  29.1 0.2 multiply_convert_fusion.1
  29.3 0.1 convert_element_type.85
  29.4 0.2 fusion.11
  29.6 0.8 copy.102
  30.4 10.0 %all-to-all-start = ((bf16[16,64,128]{2,1,0:T(8,128)(2,1)}), bf16[16,64,128]{2,1,0:T(8,128)(2,1)S(1)}, u32[]{:S(2)}, u32[]{:S(2)}) async-start(bf16[16,64,128]{2,1,0:T(8,128)(2,1)} %bitcast.53), calls=%async_computation | async-start | bytes 524288 | tf_op jit(solution)/shard_map/all_to_all | solution.py:23
  40.4 0.1 copy.81
  40.5 0.1 eq.20
  40.7 0.1 fusion.15
  40.8 0.2 reduce_window_sum.11
  40.9 0.2 select_reduce_fusion.1
  41.1 0.1 reduce_sum.107
  41.3 0.1 copy.82
  41.3 10.6 %all-to-all-done = bf16[16,64,128]{2,1,0:T(8,128)(2,1)S(1)} async-done(((bf16[16,64,128]{2,1,0:T(8,128)(2,1)}), bf16[16,64,128]{2,1,0:T(8,128)(2,1)S(1)}, u32[]{:S(2)}, u32[]{:S(2)}) %all-to-all-start) | async-done | bytes 262176 | tf_op jit(solution)/shard_map/all_to_all | solution.py:23
  52.0 0.1 fusion.16
  52.1 0.6 broadcast_in_dim.12
  52.7 3.4 %all-to-all-start.1 = ((f32[16,1,64]{2,1,0:T(1,128)}), f32[16,1,64]{2,1,0:T(1,128)S(1)}, u32[]{:S(2)}, u32[]{:S(2)}) async-start(f32[16,1,64]{2,1,0:T(1,128)} %broadcast_in_dim.12), calls=%async_computation.1 | async-start | bytes 16384 | tf_op jit(solution)/shard_map/all_to_all | solution.py:29
  56.1 0.1 fusion.14
  56.2 0.8 dynamic_slice.7
  57.0 5.7 %all-to-all-done.1 = f32[16,1,64]{2,1,0:T(1,128)S(1)} async-done(((f32[16,1,64]{2,1,0:T(1,128)}), f32[16,1,64]{2,1,0:T(1,128)S(1)}, u32[]{:S(2)}, u32[]{:S(2)}) %all-to-all-start.1) | async-done | bytes 4128 | tf_op jit(solution)/shard_map/all_to_all | solution.py:29
  62.7 0.2 convolution_convert_fusion.3
  63.0 13.1 %all_to_all.26 = bf16[16,12,128]{2,1,0:T(8,128)(2,1)S(1)} all-to-all(bf16[16,12,128]{2,1,0:T(8,128)(2,1)S(1)} %reshape.112), channel_id=1, replica_groups=mesh['ep'=16,'tp_0'=8,'tp_1'=2] {'ep'}, dimensions={0} | all-to-all | bytes 98304 | tf_op jit(solution)/shard_map/all_to_all | solution.py:167
  76.1 3.6 %all_gather.6 = bf16[192,256]{1,0:T(8,128)(2,1)S(1)} all-gather(bf16[192,128]{1,0:T(8,128)(2,1)S(1)} %reshape.113), channel_id=1, replica_groups=mesh['ep'=16,'tp_0'=8,'tp_1'=2] {'tp_1'}, dimensions={1}, use_global_device_ids=true | all-gather | bytes 147456 | tf_op jit(solution)/shard_map/all_gather | solution.py:39
  79.7 20.6 %all_gather.7 = bf16[192,2048]{1,0:T(8,128)(2,1)S(1)} all-gather(bf16[192,256]{1,0:T(8,128)(2,1)S(1)} %all_gather.6), channel_id=1, replica_groups=mesh['ep'=16,'tp_0'=8,'tp_1'=2] {'tp_0'}, dimensions={1}, use_global_device_ids=true | all-gather | bytes 884736 | tf_op jit(solution)/shard_map/all_gather | solution.py:39
  100.4 2.2 %fusion.3 = f32[192,448]{1,0:T(8,128)S(1)} fusion(bf16[192,2048]{1,0:T(8,128)(2,1)S(1)} %all_gather.7, bf16[1,2048,448]{1,2,0:T(8,128)(2,1)} %param.35), kind=kOutput, calls=%fused_computation.7 | convolution fusion | flops 352321536 | bytes 2965504 | tf_op jit(solution)/shard_map/dot_general | solution.py:178
  102.5 2.2 %fusion.8 = bf16[192,448]{1,0:T(8,128)(2,1)S(1)} fusion(bf16[192,2048]{1,0:T(8,128)(2,1)S(1)} %all_gather.7, bf16[1,2048,448]{1,2,0:T(8,128)(2,1)} %param.36, f32[192,448]{1,0:T(8,128)S(1)} %fusion.3), kind=kOutput, calls=%fused_computation.10 | convolution fusion | flops 352837632 | bytes 3137536 | tf_op jit(solution)/shard_map/dot_general | solution.py:179
  104.7 0.0 copy-start.6
  104.7 0.1 dot_general.52
  104.8 0.0 copy-done
  104.8 0.6 convolution_convert_fusion
  105.5 1.4 copy.85
  106.9 3.7 %all-to-all-start.3 = ((bf16[16,12,2048]{2,1,0:T(8,128)(2,1)}), bf16[16,12,2048]{2,1,0:T(8,128)(2,1)S(1)}, u32[]{:S(2)}, u32[]{:S(2)}) async-start(bf16[16,12,2048]{2,1,0:T(8,128)(2,1)} %copy.85), calls=%async_computation.3 | async-start | bytes 2097152 | tf_op jit(solution)/shard_map/all_to_all | solution.py:182
  110.6 0.1 select_reduce_fusion
  110.7 12.3 %all-to-all-done.3 = bf16[16,12,2048]{2,1,0:T(8,128)(2,1)S(1)} async-done(((bf16[16,12,2048]{2,1,0:T(8,128)(2,1)}), bf16[16,12,2048]{2,1,0:T(8,128)(2,1)S(1)}, u32[]{:S(2)}, u32[]{:S(2)}) %all-to-all-start.3) | async-done | bytes 786464 | tf_op jit(solution)/shard_map/all_to_all | solution.py:182
  123.0 1.1 reshape.114
  124.0 1.7 %fusion.12 = bf16[8,16,8,128]{3,2,1,0:T(8,128)(2,1)S(1)} fusion(f32[64,192]{1,0:T(8,128)S(1)} %select_reduce_fusion, bf16[192,2048]{1,0:T(8,128)(2,1)} %reshape.114), kind=kOutput, calls=%fused_computation.12 | convolution fusion | flops 302120960 | bytes 1097728 | tf_op jit(solution)/shard_map/dot_general | solution.py:189
  125.7 0.1 copy.101
  125.8 21.0 %all_to_all.27 = bf16[16,64,128]{2,1,0:T(8,128)(2,1)S(1)} all-to-all(bf16[16,64,128]{2,1,0:T(8,128)(2,1)S(1)} %bitcast.57), channel_id=1, replica_groups=mesh['ep'=16,'tp_0'=8,'tp_1'=2] {'tp_0','tp_1'}, dimensions={0} | all-to-all | bytes 524288 | tf_op jit(solution)/shard_map/all_to_all | solution.py:23
  146.8 0.6 fusion.19
  (24 shorter events, 0.3 us)
Async XLA Ops:
  0.6 104.2 %copy-start = (bf16[1,448,2048]{2,1,0:T(8,128)(2,1)S(1)}, bf16[1,448,2048]{2,1,0:T(8,128)(2,1)}, u32[]{:S(2)}) copy-start(bf16[1,448,2048]{2,1,0:T(8,128)(2,1)} %param.37) | copy-start | bytes 5505028
  11.8 8.6 %copy-start.1 = (f32[64,2,64,64]{3,2,1,0:T(8,128)S(1)}, f32[64,2,64,64]{3,2,1,0:T(8,128)}, u32[]{:S(2)}) copy-start(f32[64,2,64,64]{3,2,1,0:T(8,128)} %param.20) | copy-start | bytes 6291460
  23.2 2.0 %copy-start.2 = (f32[64,2,64,64]{3,2,1,0:T(8,128)}, f32[64,2,64,64]{3,2,1,0:T(8,128)S(1)}, u32[]{:S(2)}) copy-start(f32[64,2,64,64]{3,2,1,0:T(8,128)S(1)} %multiply_add_fusion) | copy-start | bytes 6291460
  25.2 3.8 %copy-start.7 = (f32[128]{0:T(128)S(1)}, f32[128]{0:T(128)}, u32[]{:S(2)}) copy-start(f32[128]{0:T(128)} %param.32) | copy-start | bytes 1540
  25.2 4.2 %copy-start.4 = (bf16[128,2048]{1,0:T(8,128)(2,1)S(1)}, bf16[128,2048]{1,0:T(8,128)(2,1)}, u32[]{:S(2)}) copy-start(bf16[128,2048]{1,0:T(8,128)(2,1)} %param.33) | copy-start | bytes 1572868
  25.2 15.1 %copy-start.3 = (bf16[64,2048]{1,0:T(8,128)(2,1)S(1)}, bf16[64,2048]{1,0:T(8,128)(2,1)}, u32[]{:S(2)}) copy-start(bf16[64,2048]{1,0:T(8,128)(2,1)} %param.19) | copy-start | bytes 786436
  25.2 15.2 %copy-start.5 = (s32[64,2]{0,1:T(2,128)S(1)}, s32[64,2]{0,1:T(2,128)}, u32[]{:S(2)}) copy-start(s32[64,2]{0,1:T(2,128)} %param.21) | copy-start | bytes 1540
  30.4 21.6 %all-to-all-start = ((bf16[16,64,128]{2,1,0:T(8,128)(2,1)}), bf16[16,64,128]{2,1,0:T(8,128)(2,1)S(1)}, u32[]{:S(2)}, u32[]{:S(2)}) async-start(bf16[16,64,128]{2,1,0:T(8,128)(2,1)} %bitcast.53), calls=%async_computation | async-start | bytes 524288 | tf_op jit(solution)/shard_map/all_to_all | solution.py:23
  52.7 10.0 %all-to-all-start.1 = ((f32[16,1,64]{2,1,0:T(1,128)}), f32[16,1,64]{2,1,0:T(1,128)S(1)}, u32[]{:S(2)}, u32[]{:S(2)}) async-start(f32[16,1,64]{2,1,0:T(1,128)} %broadcast_in_dim.12), calls=%async_computation.1 | async-start | bytes 16384 | tf_op jit(solution)/shard_map/all_to_all | solution.py:29
  104.7 5.8 %copy-start.6 = (f32[64,2]{0,1:T(2,128)S(1)}, f32[64,2]{0,1:T(2,128)}, u32[]{:S(2)}) copy-start(f32[64,2]{0,1:T(2,128)} %param.22) | copy-start | bytes 1540
  106.9 16.1 %all-to-all-start.3 = ((bf16[16,12,2048]{2,1,0:T(8,128)(2,1)}), bf16[16,12,2048]{2,1,0:T(8,128)(2,1)S(1)}, u32[]{:S(2)}, u32[]{:S(2)}) async-start(bf16[16,12,2048]{2,1,0:T(8,128)(2,1)} %copy.85), calls=%async_computation.3 | async-start | bytes 2097152 | tf_op jit(solution)/shard_map/all_to_all | solution.py:182
where the time goes:
time: 148 us; the launch traced here: 147 us
  blocking collectives  58.4 us (39%)
  waiting for transfers between devices  28.6 us (19%)
  matrix products  26 us (18%)
  starting transfers between devices  17 us (11%)
  local copies, waits for them, and re-layouts  8.66 us (6%)
  other arithmetic  7.79 us (5%)
    all_gather x2, blocking collectives, gather_axes(): shard = lax.all_gather(shard, axis, axis=dim, tiled=True)  24.3 us
    all_to_all x1, blocking collectives, sum_at_owner(): lax.all_to_all(pieces, axis, split_axis=0, concat_axis=0, tiled=True)  21 us
    all_to_all x1, blocking collectives, local(): lax.all_to_all(outgoing.reshape(group_count, capacity, share_cols), 'ep',...  13.1 us
    all_to_all x1, waiting for transfers between devices, local(): lax.all_to_all(expert_part.reshape(group_count, capacity, full_width).ast...  12.3 us
    all_to_all x1, waiting for transfers between devices, sum_at_owner(): lax.all_to_all(pieces, axis, split_axis=0, concat_axis=0, tiled=True)  10.6 us
    all_to_all x1, starting transfers between devices, sum_at_owner(): lax.all_to_all(pieces, axis, split_axis=0, concat_axis=0, tiled=True)  9.97 us
    dot_general x1, matrix products, mix_heads(): removed = jnp.einsum('bhvk,bhk->bhv', state, unit_key, precision=HIGHEST)  8.46 us
    dot_general x5, matrix products, project(): return rounded(jnp.dot(normed, weight, preferred_element_type=jnp.float32))  7.09 us
  transfers between devices with their start and end apart: 3, of which 3 were waited for; matrix products, arithmetic and copies ran while one was open for 1% of the time, Pallas kernels for 0%

commit v1 on v0

v1 whole, which is shorter than its diff:
```python
import jax
import jax.numpy as jnp
from jax import lax
from jax.experimental import pallas as pl
from jax.experimental.pallas import tpu as pltpu
from jax.sharding import PartitionSpec as P

MESH = pl.DeviceIdType.MESH
RMS_EPS = 1e-06
GROUP_EPS = 0.00064
UNIT_EPS = 6.4e-05
F32 = jnp.float32
BF16 = jnp.bfloat16

LANES = 128
HALF = 64
SIDE = 4
CHUNKS = 8
MAIN = 8
REST = 4

NEAR = sorted(range(SIDE * SIDE), key=lambda o: sum(min(d, SIDE - d) for d in divmod(o, SIDE)))


def dot(a, b, contract=((1,), (0,))):
    return lax.dot_general(a, b, (contract, ((), ())), preferred_element_type=F32)


def mixer_kernel(
    tok_hbm,
    st_hbm,
    mix_gain,
    w_recept,
    w_key,
    w_value,
    w_decay,
    w_rate,
    decay_base,
    rate_base,
    key_gain,
    group_gain,
    mixed_ref,
    ns_hbm,
    tok_v,
    w_v,
    st_v,
    ns_v,
    rows_v,
    read_v,
    tok_sem,
    w_sem,
    st_sem,
    ns_sem,
):
    seqs = tok_v.shape[0]
    per = seqs // CHUNKS
    tok_copy = pltpu.make_async_copy(tok_hbm, tok_v, tok_sem)
    tok_copy.start()
    w_copies = []
    for j, w_hbm in enumerate((w_recept, w_key, w_value, w_decay, w_rate)):
        copy = pltpu.make_async_copy(w_hbm, w_v.at[:, pl.ds(j * LANES, LANES)], w_sem.at[j])
        copy.start()
        w_copies.append(copy)

    def st_copy(i):
        part = pl.ds(i * per, per)
        return pltpu.make_async_copy(st_hbm.at[part], st_v.at[part], st_sem.at[i])

    def ns_copy(i):
        part = pl.ds(i * per, per)
        return pltpu.make_async_copy(ns_v.at[part], ns_hbm.at[part], ns_sem.at[i])

    for i in range(CHUNKS):
        st_copy(i).start()

    lane = lax.broadcasted_iota(jnp.int32, (seqs, LANES), 1)

    def per_head(values):
        first = jnp.sum(jnp.where(lane < HALF, values, 0.0), axis=1, keepdims=True)
        second = jnp.sum(jnp.where(lane < HALF, 0.0, values), axis=1, keepdims=True)
        return jnp.where(lane < HALF, first, second)

    tok_copy.wait()
    values = tok_v[...].astype(F32)
    scale = lax.rsqrt(jnp.mean(values * values, axis=1, keepdims=True) + RMS_EPS)
    normed = (values * scale * mix_gain[...]).astype(BF16)
    for copy in w_copies:
        copy.wait()
    projected = dot(normed, w_v[...]).astype(BF16).astype(F32)
    recept, key, value, decay_in, rate_in = (
        projected[:, j * LANES : (j + 1) * LANES] for j in range(5)
    )
    decay = jnp.exp(-(0.6065306597126334 * jax.nn.sigmoid(decay_in + decay_base[...])))
    rate = jax.nn.sigmoid(rate_in + rate_base[...])
    scaled = key * key_gain[...]
    unit = scaled * lax.rsqrt(per_head(scaled * scaled) + UNIT_EPS)
    rows_v[0] = unit
    rows_v[1] = decay
    rows_v[2] = unit * rate
    rows_v[3] = key
    rows_v[4] = recept
    rows_v[5] = value

    wide = 2 * LANES
    block_r = lax.broadcasted_iota(jnp.int32, (wide, wide), 0) // HALF
    block_c = lax.broadcasted_iota(jnp.int32, (wide, wide), 1) // HALF
    ones2 = (block_r == block_c).astype(BF16)
    ones1 = ones2[:LANES, :LANES]
    diag = (
        lax.broadcasted_iota(jnp.int32, (HALF, LANES), 0)
        == lax.broadcasted_iota(jnp.int32, (HALF, LANES), 1) % HALF
    )[None]

    def chunk(i, carry):
        st_copy(i).wait()
        part = pl.ds(pl.multiple_of(i * per, per), per)
        old = jnp.concatenate([st_v[part, 0], st_v[part, 1]], axis=-1)
        unit_c, decay_c, take_c, key_c, recept_c, value_c = (
            rows_v[j, part][:, None, :] for j in range(6)
        )
        probe = (old * unit_c).astype(BF16).reshape(per * HALF, LANES)
        spread = jnp.where(diag, value_c, 0.0).astype(BF16).reshape(per * HALF, LANES)
        both = dot(jnp.concatenate([probe, spread], axis=1), ones2)
        removed = both[:, :LANES].reshape(per, HALF, LANES)
        value_b = both[:, LANES:].reshape(per, HALF, LANES)
        new = old * decay_c - removed * take_c + value_b * key_c
        ns_v[part, 0] = new[..., :HALF]
        ns_v[part, 1] = new[..., HALF:]
        ns_copy(i).start()
        seen = dot((new * recept_c).astype(BF16).reshape(per * HALF, LANES), ones1)
        seen = jnp.where(diag, seen.reshape(per, HALF, LANES), 0.0)
        read_v[part, :] = jnp.sum(seen, axis=1)
        return carry

    lax.fori_loop(0, CHUNKS, chunk, 0)
    readout = read_v[...]
    centred = readout - per_head(readout) * (1.0 / HALF)
    spread = per_head(centred * centred) * (1.0 / HALF)
    mixed_ref[...] = (centred * lax.rsqrt(spread + GROUP_EPS) * group_gain[...]).astype(BF16)
    for i in range(CHUNKS):
        ns_copy(i).wait()


def expert_kernel(
    mixed_ref,
    tok_ref,
    routes_ref,
    logits_ref,
    gain_ref,
    wo_hbm,
    wg_hbm,
    wu_hbm,
    wd_hbm,
    out_ref,
    wo_v,
    wg_v,
    wu_v,
    wd_v,
    pair_send,
    pair_recv,
    own_v,
    rs_send,
    rs_recv,
    resid_v,
    disp_send,
    x_recv,
    xs_v,
    y_send,
    y_recv,
    yown_v,
    ret_send,
    ret_recv,
    moe_send,
    moe_recv,
    w_sem,
    wo_sem,
    wd_sem,
    pair_sem,
    rs_ssem,
    rs_rsem,
    ag_ssem,
    ag_rsem,
    disp_ssem,
    disp_rsem,
    relay_ssem,
    relay_rsem,
    y_sem,
    ret_ssem,
    ret_rsem,
    moe_ssem,
    moe_rsem,
):
    depth = lax.axis_size("tp") // 2
    rows = tok_ref.shape[0]
    groups = SIDE * SIDE
    ep = lax.axis_index("ep")
    tp = lax.axis_index("tp")
    z, core = tp // 2, tp % 2
    y, x = ep // SIDE, ep % SIDE
    other = 1 - core

    def along(dz):
        return (ep, ((z + dz) % depth) * 2 + core)

    def plane(o, sign):
        dy, dx = divmod(o, SIDE)
        to_y = (y + sign * dy + SIDE) % SIDE
        to_x = (x + sign * dx + SIDE) % SIDE
        return (to_y * SIDE + to_x, tp)

    partner = (ep, z * 2 + other)

    def send(src, dst, ssem, rsem, target):
        return pltpu.make_async_remote_copy(
            src_ref=src,
            dst_ref=dst,
            send_sem=ssem,
            recv_sem=rsem,
            device_id=target,
            device_id_type=MESH,
        )

    barrier = pltpu.get_barrier_semaphore()
    peers = [partner] + [along(dz) for dz in range(1, depth)]
    peers += [plane(o, 1) for o in range(1, groups)]
    for peer in peers:
        pl.semaphore_signal(barrier, inc=1, device_id=peer, device_id_type=MESH)

    wo_copies, wd_copies = [], []
    for j in range(2 * depth):
        cols = pl.ds(j * LANES, LANES)
        half = pl.ds((j // 2) * LANES, LANES)
        copy = pltpu.make_async_copy(wo_hbm.at[:, cols], wo_v.at[j % 2, :, half], wo_sem.at[j])
        copy.start()
        wo_copies.append(copy)
    gate_copy = pltpu.make_async_copy(wg_hbm, wg_v, w_sem.at[0])
    up_copy = pltpu.make_async_copy(wu_hbm, wu_v, w_sem.at[1])
    gate_copy.start()
    up_copy.start()
    for j in range(2 * depth):
        cols = pl.ds(j * LANES, LANES)
        half = pl.ds((j // 2) * LANES, LANES)
        copy = pltpu.make_async_copy(wd_hbm.at[:, cols], wd_v.at[j % 2, :, half], wd_sem.at[j])
        copy.start()
        wd_copies.append(copy)

    for copy in wo_copies:
        copy.wait()
    mixed = mixed_ref[...]
    theirs = dot(mixed, wo_v[other]).astype(BF16)
    for k in range(depth):
        pair_send[k] = theirs[:, k * LANES : (k + 1) * LANES]
    pl.semaphore_wait(barrier, len(peers))
    pair_copy = send(pair_send, pair_recv, pair_sem.at[0], pair_sem.at[1], partner)
    pair_copy.start()
    mine = dot(mixed, wo_v[core])
    for k in range(depth):
        own_v[k] = mine[:, k * LANES : (k + 1) * LANES]
    pair_copy.wait_recv()

    far = sorted(range(1, depth), key=lambda dz: -min(dz, depth - dz))
    rs_copies = {}
    for dz in far:
        k = (z + dz) % depth
        rs_send[dz] = (own_v[k] + pair_recv[k].astype(F32)).astype(BF16)
        copy = send(rs_send.at[dz], rs_recv.at[dz], rs_ssem.at[dz], rs_rsem.at[dz], along(dz))
        copy.start()
        rs_copies[dz] = copy
    cols = pl.ds(pl.multiple_of(tp * LANES, LANES), LANES)
    total = own_v[z] + pair_recv[z].astype(F32)

    row16 = lax.broadcasted_iota(jnp.int32, (groups, rows), 0)
    expert = (((y + (row16 >> 2)) & 3) << 2) | ((x + (row16 & 3)) & 3)
    first = (routes_ref[0:1, :] == expert).astype(BF16)
    second = (routes_ref[1:2, :] == expert).astype(BF16)
    before = (
        lax.broadcasted_iota(jnp.int32, (rows, rows), 0)
        < lax.broadcasted_iota(jnp.int32, (rows, rows), 1)
    ).astype(BF16)
    rank = dot(first + second, before).astype(BF16)
    slots = groups * MAIN
    expand = (
        (lax.broadcasted_iota(jnp.int32, (slots, groups), 0) // MAIN)
        == lax.broadcasted_iota(jnp.int32, (slots, groups), 1)
    ).astype(BF16)
    first_x = dot(expand, first)
    second_x = dot(expand, second)
    rank_x = dot(expand, rank).astype(jnp.int32)
    slot = lax.broadcasted_iota(jnp.int32, (slots, rows), 0) % MAIN
    named = (first_x + second_x) > 0.5
    pick_main = jnp.where(named & (rank_x == slot), 1.0, 0.0)
    pick_low = jnp.where(named & (rank_x == slot + MAIN) & (slot < REST), 1.0, 0.0)
    pick_high = jnp.where(named & (rank_x == slot + REST) & (slot >= REST), 1.0, 0.0)
    exp0 = jnp.exp(logits_ref[0:1, :])
    exp1 = jnp.exp(logits_ref[1:2, :])
    weight = (first_x * exp0 + second_x * exp1) / (exp0 + exp1)

    def split(table):
        turned = (table * weight).T
        top = turned.astype(BF16)
        return top, (turned - top.astype(F32)).astype(BF16)

    give_main, give_low, give_high = split(pick_main), split(pick_low), split(pick_high)
    pick_main, pick_low, pick_high = (t.astype(BF16) for t in (pick_main, pick_low, pick_high))

    for dz in reversed(far):
        rs_copies[dz].wait_recv()
        total = total + rs_recv[dz].astype(F32)
    own_resid = (tok_ref[:, cols].astype(F32) + total).astype(BF16)
    resid_v[z] = own_resid
    ag_copies = []
    for dz in far:
        copy = send(resid_v.at[z], resid_v.at[z], ag_ssem.at[dz], ag_rsem.at[dz], along(dz))
        copy.start()
        ag_copies.append(copy)
    for dz in reversed(far):
        src = resid_v.at[(z - dz + depth) % depth]
        send(src, src, ag_ssem.at[dz], ag_rsem.at[dz], along(dz)).wait_recv()

    half_cols = depth * LANES
    quarter = half_cols // 2
    resid = jnp.concatenate([resid_v[k] for k in range(depth)], axis=1)
    picked = dot(pick_main, resid).astype(BF16).reshape(groups, MAIN, half_cols)
    low = dot(pick_low, resid[:, :quarter]) + dot(pick_high, resid[:, quarter:])
    low = low.astype(BF16).reshape(groups, MAIN, quarter)
    disp_send[:, :, 0:half_cols] = picked
    disp_send[:, :, half_cols:] = low
    x_recv[core, 0] = disp_send[0]
    disp_copies = {}
    for o in reversed(NEAR[1:]):
        copy = send(
            disp_send.at[o], x_recv.at[core, o], disp_ssem.at[o], disp_rsem.at[o], plane(o, 1)
        )
        copy.start()
        disp_copies[o] = copy
    relays = []
    for o in NEAR:
        src = disp_send.at[0]
        if o:
            disp_copies[o].wait_recv()
            src = x_recv.at[core, o]
        copy = send(src, x_recv.at[core, o], relay_ssem.at[o], relay_rsem.at[o], partner)
        copy.start()
        relays.append(copy)
    for o in NEAR:
        dst = x_recv.at[other, o]
        send(dst, dst, relay_ssem.at[o], relay_rsem.at[o], partner).wait_recv()

    main_rows = groups * MAIN
    all_rows = main_rows + groups * REST
    tile_row = lax.broadcasted_iota(jnp.int32, (groups // 2, MAIN, quarter), 1)
    upper = tile_row < REST
    halves_main, halves_rest = [], []
    for p in range(2):
        block = x_recv[p].astype(F32)
        halves_main.append(block[:, :, :half_cols].reshape(main_rows, half_cols))
        rest = block[:, :, half_cols:].reshape(groups // 2, 2, MAIN, quarter)
        a, b = rest[:, 0], rest[:, 1]
        lower_cols = jnp.where(upper, a, pltpu.roll(b, REST, 1))
        upper_cols = jnp.where(upper, pltpu.roll(a, REST, 1), b)
        joined = jnp.concatenate([lower_cols, upper_cols], axis=2)
        halves_rest.append(joined.reshape(all_rows - main_rows, half_cols))
    width = 2 * half_cols
    for start, halves in ((0, halves_main), (main_rows, halves_rest)):
        count = halves[0].shape[0]
        squares = sum(jnp.sum(h * h, axis=1, keepdims=True) for h in halves)
        scale = lax.rsqrt(squares * (1.0 / width) + RMS_EPS)
        for p in range(2):
            for k in range(depth):
                at = (2 * k + p) * LANES
                piece = halves[p][:, k * LANES : (k + 1) * LANES] * scale
                piece = piece * gain_ref[:, at : at + LANES]
                xs_v[start : start + count, at : at + LANES] = piece.astype(BF16)

    gate_copy.wait()
    up_copy.wait()
    for copy in wd_copies:
        copy.wait()
    xs = xs_v[...]
    gate = dot(xs, wg_v[...], ((1,), (1,)))
    up = dot(xs, wu_v[...], ((1,), (1,)))
    hidden = (gate * jax.nn.sigmoid(gate) * up).astype(BF16)
    y_send[...] = dot(hidden, wd_v[other]).astype(BF16)
    y_copy = send(y_send, y_recv, y_sem.at[0], y_sem.at[1], partner)
    y_copy.start()
    yown_v[...] = dot(hidden, wd_v[core])
    y_copy.wait_recv()

    summed = yown_v[...] + y_recv[...].astype(F32)
    ret_send[:, :, 0:half_cols] = (
        summed[:main_rows].astype(BF16).reshape(groups, MAIN, half_cols)
    )
    rest = summed[main_rows:].reshape(groups // 2, MAIN, half_cols)
    lower_cols, upper_cols = rest[:, :, :quarter], rest[:, :, quarter:]
    a = jnp.where(upper, lower_cols, pltpu.roll(upper_cols, REST, 1))
    b = jnp.where(upper, pltpu.roll(lower_cols, REST, 1), upper_cols)
    for p in range(groups // 2):
        ret_send[2 * p, :, half_cols:] = a[p].astype(BF16)
        ret_send[2 * p + 1, :, half_cols:] = b[p].astype(BF16)
    ret_recv[0] = ret_send[0]
    ret_copies = {}
    for o in reversed(NEAR[1:]):
        copy = send(ret_send.at[o], ret_recv.at[o], ret_ssem.at[o], ret_rsem.at[o], plane(o, -1))
        copy.start()
        ret_copies[o] = copy
    for o in NEAR[1:]:
        ret_copies[o].wait_recv()

    back = ret_recv[...]
    back_main = back[:, :, :half_cols].reshape(slots, half_cols)
    back_rest = back[:, :, half_cols:].reshape(slots, quarter)

    def give(tables, data):
        return dot(tables[0], data) + dot(tables[1], data)

    moe = give(give_main, back_main)
    moe_low = moe[:, :quarter] + give(give_low, back_rest)
    moe_high = moe[:, quarter:] + give(give_high, back_rest)
    moe = jnp.concatenate([moe_low, moe_high], axis=1)
    for k in range(depth):
        own_v[k] = moe[:, k * LANES : (k + 1) * LANES]
    moe_copies = {}
    for dz in far:
        moe_send[dz] = own_v[(z + dz) % depth].astype(BF16)
        copy = send(moe_send.at[dz], moe_recv.at[dz], moe_ssem.at[dz], moe_rsem.at[dz], along(dz))
        copy.start()
        moe_copies[dz] = copy
    total = own_resid.astype(F32) + own_v[z]
    for dz in reversed(far):
        moe_copies[dz].wait_recv()
        total = total + moe_recv[dz].astype(F32)
    out_ref[...] = total.astype(BF16)

    sent = [pair_copy, y_copy] + ag_copies + relays
    for group in (rs_copies, disp_copies, ret_copies, moe_copies):
        sent += list(group.values())
    for copy in sent:
        copy.wait_send()


def local(
    tokens,
    state,
    routes,
    route_logits,
    mix_gain,
    w_recept,
    w_key,
    w_value,
    w_decay,
    w_rate,
    decay_base,
    rate_base,
    key_gain,
    group_gain,
    w_output,
    ffn_gain,
    w_gate,
    w_up,
    w_down,
):
    seqs, width = tokens.shape
    hidden = w_gate.shape[2]
    vmem = pl.BlockSpec(memory_space=pltpu.VMEM)
    anywhere = pl.BlockSpec(memory_space=pl.ANY)
    dma = pltpu.SemaphoreType.DMA

    def row(vector):
        return vector.reshape(1, -1)

    mixed, new_state = pl.pallas_call(
        mixer_kernel,
        out_shape=(
            jax.ShapeDtypeStruct((seqs, LANES), BF16),
            jax.ShapeDtypeStruct(state.shape, F32),
        ),
        in_specs=[anywhere, anywhere, vmem] + [anywhere] * 5 + [vmem] * 4,
        out_specs=(vmem, anywhere),
        scratch_shapes=[
            pltpu.VMEM((seqs, width), BF16),
            pltpu.VMEM((width, 5 * LANES), BF16),
            pltpu.VMEM(state.shape, F32),
            pltpu.VMEM(state.shape, F32),
            pltpu.VMEM((6, seqs, LANES), F32),
            pltpu.VMEM((seqs, LANES), F32),
            dma(()),
            dma((5,)),
            dma((CHUNKS,)),
            dma((CHUNKS,)),
        ],
        compiler_params=pltpu.CompilerParams(vmem_limit_bytes=40 * 2**20),
        name="mixer",
    )(
        tokens,
        state,
        row(mix_gain),
        w_recept,
        w_key,
        w_value,
        w_decay,
        w_rate,
        row(decay_base),
        row(rate_base),
        row(key_gain),
        row(group_gain),
    )

    depth = lax.axis_size("tp") // 2
    groups = SIDE * SIDE
    half_cols = depth * LANES
    message = half_cols + half_cols // 2
    all_rows = groups * (MAIN + REST)
    block = (depth, seqs, LANES)
    output = pl.pallas_call(
        expert_kernel,
        out_shape=jax.ShapeDtypeStruct((seqs, LANES), BF16),
        in_specs=[vmem] * 5 + [anywhere] * 4,
        out_specs=vmem,
        scratch_shapes=[
            pltpu.VMEM((2, LANES, half_cols), BF16),
            pltpu.VMEM((hidden, width), BF16),
            pltpu.VMEM((hidden, width), BF16),
            pltpu.VMEM((2, hidden, half_cols), BF16),
            pltpu.VMEM(block, BF16),
            pltpu.VMEM(block, BF16),
            pltpu.VMEM(block, F32),
            pltpu.VMEM(block, BF16),
            pltpu.VMEM(block, BF16),
            pltpu.VMEM(block, BF16),
            pltpu.VMEM((groups, MAIN, message), BF16),
            pltpu.VMEM((2, groups, MAIN, message), BF16),
            pltpu.VMEM((all_rows, width), BF16),
            pltpu.VMEM((all_rows, half_cols), BF16),
            pltpu.VMEM((all_rows, half_cols), BF16),
            pltpu.VMEM((all_rows, half_cols), F32),
            pltpu.VMEM((groups, MAIN, message), BF16),
            pltpu.VMEM((groups, MAIN, message), BF16),
            pltpu.VMEM(block, BF16),
            pltpu.VMEM(block, BF16),
            dma((2,)),
            dma((2 * depth,)),
            dma((2 * depth,)),
            dma((2,)),
            dma((depth,)),
            dma((depth,)),
            dma((depth,)),
            dma((depth,)),
            dma((groups,)),
            dma((groups,)),
            dma((groups,)),
            dma((groups,)),
            dma((2,)),
            dma((groups,)),
            dma((groups,)),
            dma((depth,)),
            dma((depth,)),
        ],
        compiler_params=pltpu.CompilerParams(
            collective_id=0, has_side_effects=True, vmem_limit_bytes=48 * 2**20
        ),
        name="experts",
    )(
        mixed,
        tokens,
        routes.T,
        route_logits.T,
        row(ffn_gain),
        w_output,
        jnp.swapaxes(w_gate, 1, 2)[0],
        jnp.swapaxes(w_up, 1, 2)[0],
        w_down[0],
    )
    return (output, new_state)


def solution(mesh):
    return jax.shard_map(
        local,
        mesh=mesh,
        in_specs=(
            P("ep", None),
            P("ep", "tp", None, None),
            P("ep", None),
            P("ep", None),
            P(),
            P(None, "tp"),
            P(None, "tp"),
            P(None, "tp"),
            P(None, "tp"),
            P(None, "tp"),
            P("tp"),
            P("tp"),
            P("tp"),
            P("tp"),
            P("tp", None),
            P(),
            P("ep", None, "tp"),
            P("ep", None, "tp"),
            P("ep", "tp", None),
        ),
        out_specs=(P("ep", "tp"), P("ep", "tp", None, None)),
        check_vma=False,
    )
```

time: 148 us -> 66.4 us (0.45)
  blocking collectives: 58.4 us -> 0 us
  Pallas kernels: 0 us -> 52.9 us
  waiting for transfers between devices: 28.6 us -> 0 us
  matrix products: 26 us -> 0 us
  starting transfers between devices: 17 us -> 0 us
  other arithmetic: 7.79 us -> 0 us
  local copies, waits for them, and re-layouts: 8.66 us -> 12.3 us
    pallas_call x0 -> x2, Pallas kernels: none -> 52.9 us  [the longest x1 46.9 us: local(): pl.pallas_call(expert_kernel, out_shape=jax.ShapeDtypeStruct((seqs, LANES...]
    all_to_all x2 -> x0, blocking collectives: 34.1 us -> none  [the longest x1 21 us: sum_at_owner(): lax.all_to_all(pieces, axis, split_axis=0, concat_axis=0, tiled=True)]
    all_to_all x3 -> x0, waiting for transfers between devices: 28.6 us -> none  [the longest x1 12.3 us: local(): lax.all_to_all(expert_part.reshape(group_count, capacity, full_width).ast...]
    dot_general x13 -> x0, matrix products: 26 us -> none  [the longest x1 8.46 us: mix_heads(): removed = jnp.einsum('bhvk,bhk->bhv', state, unit_key, precision=HIGHEST)]
    all_gather x2 -> x0, blocking collectives: 24.3 us -> none  [gather_axes(): shard = lax.all_gather(shard, axis, axis=dim, tiled=True)]
    all_to_all x3 -> x0, starting transfers between devices: 17 us -> none  [the longest x1 9.97 us: sum_at_owner(): lax.all_to_all(pieces, axis, split_axis=0, concat_axis=0, tiled=True)]
    unnamed x17 -> x39, local copies, waits for them, and re-layouts: 2.14 us -> 12.3 us
    add x2 -> x0, other arithmetic: 2.75 us -> none  [the longest x1 2.75 us: mix_heads(): state * decay_now[:, :, None, :]]
  transfers between devices with their start and end apart: 3 -> 0, of which waited for: 3 -> 0; matrix products, arithmetic and copies ran while one was open for 1% -> 0% of each run, Pallas kernels for 0% -> 0%
where the time goes in v1:
time: 66.4 us; the launch traced here: 65.9 us
  Pallas kernels  52.9 us (80%)
  local copies, waits for them, and re-layouts  12.3 us (19%)
  between operations  0.76 us (1%)
    pallas_call x1, Pallas kernels, local(): pl.pallas_call(expert_kernel, out_shape=jax.ShapeDtypeStruct((seqs, LANES...  46.9 us
    unnamed x39, local copies, waits for them, and re-layouts  12.3 us
    pallas_call x1, Pallas kernels, local(): pl.pallas_call(mixer_kernel, out_shape=(jax.ShapeDtypeStruct((seqs, LANES...  6.01 us

profile of v1, /device:TPU:1, one launch (start us, length us, event | category | flops | bytes accessed | tf_op | source)
XLA Modules:
  0.0 65.9 jit_solution(5380449322449131755)
XLA Ops:
  0.6 0.0 copy-start
  0.6 2.2 %copy-done = f32[64,2,64,64]{3,2,1,0:T(8,128)S(1)} copy-done((f32[64,2,64,64]{3,2,1,0:T(8,128)S(1)}, f32[64,2,64,64]{3,2,1,0:T(8,128)}, u32[]{:S(2)}) %copy-start) | copy-done | bytes 2097176
  2.8 0.0 copy-start.3
  2.8 0.9 %copy-done.3 = bf16[64,2048]{1,0:T(8,128)(2,1)S(1)} copy-done((bf16[64,2048]{1,0:T(8,128)(2,1)S(1)}, bf16[64,2048]{1,0:T(8,128)(2,1)}, u32[]{:S(2)}) %copy-start.3) | copy-done | bytes 262168
  3.8 0.0 copy-start.5
  3.8 1.0 %copy-done.5 = bf16[2048,128]{1,0:T(8,128)(2,1)S(1)} copy-done((bf16[2048,128]{1,0:T(8,128)(2,1)S(1)}, bf16[2048,128]{1,0:T(8,128)(2,1)}, u32[]{:S(2)}) %copy-start.5) | copy-done | bytes 524312
  4.8 0.0 copy-start.6
  4.8 1.0 %copy-done.6 = bf16[2048,128]{1,0:T(8,128)(2,1)S(1)} copy-done((bf16[2048,128]{1,0:T(8,128)(2,1)S(1)}, bf16[2048,128]{1,0:T(8,128)(2,1)}, u32[]{:S(2)}) %copy-start.6) | copy-done | bytes 524312
  5.9 0.0 copy-start.7
  5.9 1.0 %copy-done.7 = bf16[2048,128]{1,0:T(8,128)(2,1)S(1)} copy-done((bf16[2048,128]{1,0:T(8,128)(2,1)S(1)}, bf16[2048,128]{1,0:T(8,128)(2,1)}, u32[]{:S(2)}) %copy-start.7) | copy-done | bytes 524312
  6.9 0.0 copy-start.8
  6.9 1.0 %copy-done.8 = bf16[2048,128]{1,0:T(8,128)(2,1)S(1)} copy-done((bf16[2048,128]{1,0:T(8,128)(2,1)S(1)}, bf16[2048,128]{1,0:T(8,128)(2,1)}, u32[]{:S(2)}) %copy-start.8) | copy-done | bytes 524312
  7.9 0.0 copy-start.9
  7.9 1.0 %copy-done.9 = bf16[2048,128]{1,0:T(8,128)(2,1)S(1)} copy-done((bf16[2048,128]{1,0:T(8,128)(2,1)S(1)}, bf16[2048,128]{1,0:T(8,128)(2,1)}, u32[]{:S(2)}) %copy-start.9) | copy-done | bytes 524312
  9.0 0.0 copy-start.11
  9.0 0.7 %copy-done.11 = f32[2048]{0:T(1024)S(1)} copy-done((f32[2048]{0:T(1024)S(1)}, f32[2048]{0:T(1024)}, u32[]{:S(2)}) %copy-start.11) | copy-done | bytes 8216
  9.7 0.0 copy-start.15
  9.7 0.7 copy-done.15
  10.3 0.0 copy-start.16
  10.3 0.7 copy-done.16
  11.0 0.0 copy-start.17
  11.0 0.7 copy-done.17
  11.7 0.0 copy-start.18
  11.7 0.7 copy-done.18
  12.3 0.0 copy-start.1
  12.3 0.0 copy-start.2
  12.3 0.0 copy-start.4
  12.3 0.0 copy-start.10
  12.3 0.0 copy-start.12
  12.3 0.0 copy-start.13
  12.3 0.0 copy-start.14
  12.3 6.0 %mixer.1 = (bf16[64,128]{1,0:T(8,128)(2,1)S(1)}, f32[64,2,64,64]{3,2,1,0:T(8,128)}) custom-call(bf16[64,2048]{1,0:T(8,128)(2,1)S(1)} %copy-done.3, f32[64,2,64,64]{3,2,1,0:T(8,128)S(1)} %copy-done, f32[1,2048]{1,0:T(1,128)S(1)} %bitcast.17, bf16[2048,128]{1,0:T(8,128)(2,1)S(1)} %copy-done.5, bf16[2048,128]{1,0:T(8,128)(2,1)S(1)} %copy-done.6, ...), custom_call_target="tpu_custom_call" | custom-call | tf_op jit(solution)/shard_map/mixer/pallas_call | solution.py:471
  18.4 0.0 copy-done.1
  18.4 0.0 copy-done.2
  18.4 0.0 copy-done.4
  18.4 0.0 copy-done.10
  18.4 0.0 copy-done.12
  18.4 0.0 copy-done.13
  18.4 0.0 copy-done.14
  18.4 46.9 %experts.1 = bf16[64,128]{1,0:T(8,128)(2,1)S(1)} custom-call(bf16[64,128]{1,0:T(8,128)(2,1)S(1)} %get-tuple-element.4.mixed_ref, bf16[64,2048]{1,0:T(8,128)(2,1)S(1)} %copy-done.4, s32[2,64]{1,0:T(2,128)S(1)} %bitcast.19, f32[2,64]{1,0:T(2,128)S(1)} %bitcast.20, f32[1,2048]{1,0:T(1,128)S(1)} %bitcast.18, bf16[128,2048]{1,0:T(8,128)(2,1)S(1)} %copy-done.10, ...), custom_call_target="tpu_custom_call" | custom-call | tf_op jit(solution)/shard_map/experts/pallas_call | solution.py:514
  65.3 0.6 copy.22
Async XLA Ops:
  0.6 2.2 %copy-start = (f32[64,2,64,64]{3,2,1,0:T(8,128)S(1)}, f32[64,2,64,64]{3,2,1,0:T(8,128)}, u32[]{:S(2)}) copy-start(f32[64,2,64,64]{3,2,1,0:T(8,128)} %st_hbm.1) | copy-start | bytes 6291460
  2.8 0.9 %copy-start.3 = (bf16[64,2048]{1,0:T(8,128)(2,1)S(1)}, bf16[64,2048]{1,0:T(8,128)(2,1)}, u32[]{:S(2)}) copy-start(bf16[64,2048]{1,0:T(8,128)(2,1)} %tok_ref.1) | copy-start | bytes 786436
  3.8 1.0 %copy-start.5 = (bf16[2048,128]{1,0:T(8,128)(2,1)S(1)}, bf16[2048,128]{1,0:T(8,128)(2,1)}, u32[]{:S(2)}) copy-start(bf16[2048,128]{1,0:T(8,128)(2,1)} %w_recept.1) | copy-start | bytes 1572868
  4.8 1.0 %copy-start.6 = (bf16[2048,128]{1,0:T(8,128)(2,1)S(1)}, bf16[2048,128]{1,0:T(8,128)(2,1)}, u32[]{:S(2)}) copy-start(bf16[2048,128]{1,0:T(8,128)(2,1)} %w_key.1) | copy-start | bytes 1572868
  5.9 1.0 %copy-start.7 = (bf16[2048,128]{1,0:T(8,128)(2,1)S(1)}, bf16[2048,128]{1,0:T(8,128)(2,1)}, u32[]{:S(2)}) copy-start(bf16[2048,128]{1,0:T(8,128)(2,1)} %w_value.1) | copy-start | bytes 1572868
  6.9 1.0 %copy-start.8 = (bf16[2048,128]{1,0:T(8,128)(2,1)S(1)}, bf16[2048,128]{1,0:T(8,128)(2,1)}, u32[]{:S(2)}) copy-start(bf16[2048,128]{1,0:T(8,128)(2,1)} %w_decay.1) | copy-start | bytes 1572868
  7.9 1.0 %copy-start.9 = (bf16[2048,128]{1,0:T(8,128)(2,1)S(1)}, bf16[2048,128]{1,0:T(8,128)(2,1)}, u32[]{:S(2)}) copy-start(bf16[2048,128]{1,0:T(8,128)(2,1)} %w_rate.1) | copy-start | bytes 1572868
  9.0 0.7 %copy-start.11 = (f32[2048]{0:T(1024)S(1)}, f32[2048]{0:T(1024)}, u32[]{:S(2)}) copy-start(f32[2048]{0:T(1024)} %param.23) | copy-start | bytes 24580
  9.7 0.7 copy-start.15
  10.3 0.7 copy-start.16
  11.0 0.7 copy-start.17
  11.7 0.7 copy-start.18
  12.3 6.1 %copy-start.1 = (bf16[1,2048,448]{1,2,0:T(8,128)(2,1)S(1)}, bf16[1,2048,448]{1,2,0:T(8,128)(2,1)}, u32[]{:S(2)}) copy-start(bf16[1,2048,448]{1,2,0:T(8,128)(2,1)} %param.35) | copy-start | bytes 5505028
  12.3 6.1 %copy-start.2 = (bf16[1,2048,448]{1,2,0:T(8,128)(2,1)S(1)}, bf16[1,2048,448]{1,2,0:T(8,128)(2,1)}, u32[]{:S(2)}) copy-start(bf16[1,2048,448]{1,2,0:T(8,128)(2,1)} %param.36) | copy-start | bytes 5505028
  12.3 6.1 %copy-start.4 = (bf16[64,2048]{1,0:T(8,128)(2,1)S(1)}, bf16[64,2048]{1,0:T(8,128)(2,1)}, u32[]{:S(2)}) copy-start(bf16[64,2048]{1,0:T(8,128)(2,1)} %tok_ref.1) | copy-start | bytes 786436
  12.3 6.1 %copy-start.10 = (bf16[128,2048]{1,0:T(8,128)(2,1)S(1)}, bf16[128,2048]{1,0:T(8,128)(2,1)}, u32[]{:S(2)}) copy-start(bf16[128,2048]{1,0:T(8,128)(2,1)} %wo_hbm.1) | copy-start | bytes 1572868
  12.3 6.1 %copy-start.12 = (f32[2048]{0:T(1024)S(1)}, f32[2048]{0:T(1024)}, u32[]{:S(2)}) copy-start(f32[2048]{0:T(1024)} %param.34) | copy-start | bytes 24580
  12.3 6.1 %copy-start.13 = (s32[64,2]{0,1:T(2,128)S(1)}, s32[64,2]{0,1:T(2,128)}, u32[]{:S(2)}) copy-start(s32[64,2]{0,1:T(2,128)} %param.21) | copy-start | bytes 1540
  12.3 6.1 %copy-start.14 = (f32[64,2]{0,1:T(2,128)S(1)}, f32[64,2]{0,1:T(2,128)}, u32[]{:S(2)}) copy-start(f32[64,2]{0,1:T(2,128)} %param.22) | copy-start | bytes 1540

commit v2 on v1

v2 whole, which is shorter than its diff:
```python
import jax
import jax.numpy as jnp
from jax import lax
from jax.experimental import pallas as pl
from jax.experimental.pallas import tpu as pltpu
from jax.sharding import PartitionSpec as P

MESH = pl.DeviceIdType.MESH
RMS_EPS = 1e-06
GROUP_EPS = 0.00064
UNIT_EPS = 6.4e-05
F32 = jnp.float32
BF16 = jnp.bfloat16

LANES = 128
HALF = 64
SIDE = 4
CHUNKS = 4
PAIR = 8
MAIN = 8
REST = 4
GRANT = 67043328

NEAR = sorted(range(SIDE * SIDE), key=lambda o: sum(min(d, SIDE - d) for d in divmod(o, SIDE)))


def dot(a, b, contract=((1,), (0,))):
    return lax.dot_general(a, b, (contract, ((), ())), preferred_element_type=F32)


def mixer_kernel(
    tok_hbm,
    st_hbm,
    gain_hbm,
    w_recept,
    w_key,
    w_value,
    w_decay,
    w_rate,
    decay_hbm,
    rate_hbm,
    key_hbm,
    group_hbm,
    mixed_hbm,
    ns_hbm,
    mixed_ref,
    tok_v,
    mix_gain,
    vec_v,
    w_v,
    st_v,
    ns_v,
    rows_v,
    read_v,
    tok_sem,
    gain_sem,
    vec_sem,
    w_sem,
    st_sem,
    ns_sem,
):
    seqs = tok_v.shape[0]
    per = seqs // CHUNKS
    tok_copy = pltpu.make_async_copy(tok_hbm, tok_v, tok_sem)
    tok_copy.start()
    gain_copy = pltpu.make_async_copy(gain_hbm, mix_gain, gain_sem)
    gain_copy.start()
    for j, w_hbm in enumerate((w_recept, w_key, w_value, w_decay, w_rate)):
        pltpu.make_async_copy(w_hbm, w_v.at[:, pl.ds(j * LANES, LANES)], w_sem).start()
    for j, vec_hbm in enumerate((decay_hbm, rate_hbm, key_hbm, group_hbm)):
        pltpu.make_async_copy(vec_hbm, vec_v.at[j], vec_sem).start()

    def st_copy(i):
        part = pl.ds(i * per, per)
        return pltpu.make_async_copy(st_hbm.at[part], st_v.at[part], st_sem.at[i])

    def ns_copy(i):
        part = pl.ds(i * per, per)
        return pltpu.make_async_copy(ns_v.at[part], ns_hbm.at[part], ns_sem)

    lane = lax.broadcasted_iota(jnp.int32, (seqs, LANES), 1)

    def per_head(values):
        first = jnp.sum(jnp.where(lane < HALF, values, 0.0), axis=1, keepdims=True)
        second = jnp.sum(jnp.where(lane < HALF, 0.0, values), axis=1, keepdims=True)
        return jnp.where(lane < HALF, first, second)

    tok_copy.wait()
    for i in range(CHUNKS):
        st_copy(i).start()
    values = tok_v[...].astype(F32)
    scale = lax.rsqrt(jnp.mean(values * values, axis=1, keepdims=True) + RMS_EPS)
    gain_copy.wait()
    normed = (values * scale * mix_gain[...]).astype(BF16)
    pltpu.make_async_copy(w_v, w_v, w_sem).wait()
    pltpu.make_async_copy(vec_v, vec_v, vec_sem).wait()
    decay_base, rate_base, key_gain, group_gain = (vec_v[j] for j in range(4))
    projected = dot(normed, w_v[...]).astype(BF16).astype(F32)
    recept, key, value, decay_in, rate_in = (
        projected[:, j * LANES : (j + 1) * LANES] for j in range(5)
    )
    decay = jnp.exp(-(0.6065306597126334 * jax.nn.sigmoid(decay_in + decay_base)))
    rate = jax.nn.sigmoid(rate_in + rate_base)
    scaled = key * key_gain
    unit = scaled * lax.rsqrt(per_head(scaled * scaled) + UNIT_EPS)
    rows_v[0] = unit
    rows_v[1] = decay
    rows_v[2] = unit * rate
    rows_v[3] = key
    rows_v[4] = decay * recept
    rows_v[5] = value

    wide = 2 * LANES
    block_r = lax.broadcasted_iota(jnp.int32, (wide, wide), 0) // HALF
    block_c = lax.broadcasted_iota(jnp.int32, (wide, wide), 1) // HALF
    ones2 = (block_r == block_c).astype(BF16)
    ones1 = ones2[:LANES, :LANES]
    diag = (
        lax.broadcasted_iota(jnp.int32, (HALF, LANES), 0)
        == lax.broadcasted_iota(jnp.int32, (HALF, LANES), 1) % HALF
    )[None]

    def chunk(i, carry):
        st_copy(i).wait()
        for p in range(per // PAIR):
            part = pl.ds(i * per + p * PAIR, PAIR)
            old = jnp.concatenate([st_v[part, 0], st_v[part, 1]], axis=-1)
            unit_c, decay_c, take_c, key_c, seen_c, value_c = (
                rows_v[j, part][:, None, :] for j in range(6)
            )
            probe = (old * unit_c).astype(BF16).reshape(PAIR * HALF, LANES)
            spread = jnp.where(diag, value_c, 0.0).astype(BF16).reshape(PAIR * HALF, LANES)
            both = dot(jnp.concatenate([probe, spread], axis=1), ones2)
            seen = dot((old * seen_c).astype(BF16).reshape(PAIR * HALF, LANES), ones1)
            removed = both[:, :LANES].reshape(PAIR, HALF, LANES)
            value_b = both[:, LANES:].reshape(PAIR, HALF, LANES)
            new = old * decay_c - removed * take_c + value_b * key_c
            ns_v[part, 0] = new[..., :HALF]
            ns_v[part, 1] = new[..., HALF:]
            read_v[0, part, :] = jnp.sum(jnp.where(diag, removed, 0.0), axis=1)
            seen = jnp.where(diag, seen.reshape(PAIR, HALF, LANES), 0.0)
            read_v[1, part, :] = jnp.sum(seen, axis=1)
        ns_copy(i).start()
        return carry

    lax.fori_loop(0, CHUNKS, chunk, 0)
    readout = read_v[1] - read_v[0] * per_head(unit * rate * recept) + value * per_head(key * recept)
    centred = readout - per_head(readout) * (1.0 / HALF)
    spread = per_head(centred * centred) * (1.0 / HALF)
    mixed_ref[...] = (centred * lax.rsqrt(spread + GROUP_EPS) * group_gain).astype(BF16)
    mixed_copy = pltpu.make_async_copy(mixed_ref, mixed_hbm, tok_sem)
    mixed_copy.start()
    pltpu.make_async_copy(ns_v, ns_hbm, ns_sem).wait()
    mixed_copy.wait()


def expert_kernel(
    mixed_hbm,
    tok_hbm,
    routes_hbm,
    logits_hbm,
    gain_hbm,
    wo_hbm,
    wg_hbm,
    wu_hbm,
    wd_hbm,
    out_ref,
    mixed_ref,
    tok_ref,
    routes_ref,
    logits_ref,
    gain_ref,
    wo_v,
    wg_v,
    wu_v,
    wd_v,
    pair_send,
    pair_recv,
    own_v,
    rs_send,
    rs_recv,
    resid_v,
    disp_send,
    x_recv,
    gate_v,
    up_v,
    y_send,
    y_recv,
    ret_send,
    ret_recv,
    moe_send,
    moe_recv,
    in_sem,
    w_sem,
    send_sem,
    pair_sem,
    rs_sem,
    ag_sem,
    disp_sem,
    relay_sem,
    y_sem,
    ret_sem,
    moe_sem,
):
    depth = lax.axis_size("tp") // 2
    rows = tok_ref.shape[0]
    groups = SIDE * SIDE
    ep = lax.axis_index("ep")
    tp = lax.axis_index("tp")
    z, core = tp // 2, tp % 2
    y, x = ep // SIDE, ep % SIDE
    other = 1 - core

    def up_z(dz):
        return (z + dz) % depth

    def down_z(dz):
        return (z - dz + depth) % depth

    def along(dz):
        return (ep, up_z(dz) * 2 + core)

    def plane(o, sign):
        dy, dx = divmod(o, SIDE)
        to_y = (y + sign * dy + SIDE) % SIDE
        to_x = (x + sign * dx + SIDE) % SIDE
        return (to_y * SIDE + to_x, tp)

    partner = (ep, z * 2 + other)

    def send(src, dst, sender_sem, recv_sem, target):
        pltpu.make_async_remote_copy(
            src_ref=src,
            dst_ref=dst,
            send_sem=sender_sem,
            recv_sem=recv_sem,
            device_id=target,
            device_id_type=MESH,
        ).start()

    def take(ref, sem):
        pltpu.make_async_copy(ref, ref, sem).wait()

    def fetch(src, dst, sem):
        pltpu.make_async_copy(src, dst, sem).start()

    barrier = pltpu.get_barrier_semaphore()
    peers = [partner] + [along(dz) for dz in range(1, depth)]
    peers += [plane(o, 1) for o in range(1, groups)]
    for peer in peers:
        pl.semaphore_signal(barrier, inc=1, device_id=peer, device_id_type=MESH)

    fetch(mixed_hbm, mixed_ref, in_sem.at[0])
    for j in range(2 * depth):
        fetch(wo_hbm.at[:, pl.ds(j * LANES, LANES)], wo_v.at[j % 2, j // 2], in_sem.at[1])
    own_cols = pl.ds(pl.multiple_of(tp * LANES, LANES), LANES)
    fetch(routes_hbm, routes_ref, in_sem.at[2])
    fetch(logits_hbm, logits_ref, in_sem.at[3])
    fetch(tok_hbm.at[:, own_cols], tok_ref, in_sem.at[4])
    fetch(gain_hbm, gain_ref, in_sem.at[5])

    take(mixed_ref, in_sem.at[0])
    take(wo_v, in_sem.at[1])
    fetch(wg_hbm, wg_v, w_sem.at[0])
    fetch(wu_hbm, wu_v, w_sem.at[1])
    for j in range(2 * depth):
        fetch(wd_hbm.at[:, pl.ds(j * LANES, LANES)], wd_v.at[j % 2, j // 2], w_sem.at[2])

    mixed = mixed_ref[...]

    def wide(ref, side, blocks):
        return jnp.concatenate([ref[side, k] for k in blocks], axis=1)

    theirs = dot(mixed, wide(wo_v, other, range(depth))).astype(BF16)
    for k in range(depth):
        pair_send[k] = theirs[:, k * LANES : (k + 1) * LANES]
    pl.semaphore_wait(barrier, len(peers))
    send(pair_send, pair_recv, send_sem.at[0], pair_sem, partner)
    mine = dot(mixed, wide(wo_v, core, range(depth)))
    for k in range(depth):
        own_v[k] = mine[:, k * LANES : (k + 1) * LANES]
    take(pair_recv, pair_sem)

    far = sorted(range(1, depth), key=lambda dz: -min(dz, depth - dz))
    for dz in far:
        k = up_z(dz)
        rs_send[dz] = (own_v[k] + pair_recv[k].astype(F32)).astype(BF16)
        send(rs_send.at[dz], rs_recv.at[dz], send_sem.at[1], rs_sem, along(dz))
    total = own_v[z] + pair_recv[z].astype(F32)

    for j, ref in enumerate((routes_ref, logits_ref, tok_ref, gain_ref)):
        take(ref, in_sem.at[2 + j])
    row16 = lax.broadcasted_iota(jnp.int32, (groups, rows), 0)
    expert = (((y + (row16 >> 2)) & 3) << 2) | ((x + (row16 & 3)) & 3)
    first = (routes_ref[0:1, :] == expert).astype(BF16)
    second = (routes_ref[1:2, :] == expert).astype(BF16)
    before = (
        lax.broadcasted_iota(jnp.int32, (rows, rows), 0)
        < lax.broadcasted_iota(jnp.int32, (rows, rows), 1)
    ).astype(BF16)
    rank = dot(first + second, before).astype(BF16)
    slots = groups * MAIN
    expand = (
        (lax.broadcasted_iota(jnp.int32, (slots, groups), 0) // MAIN)
        == lax.broadcasted_iota(jnp.int32, (slots, groups), 1)
    ).astype(BF16)
    first_x = dot(expand, first)
    second_x = dot(expand, second)
    rank_x = dot(expand, rank).astype(jnp.int32)
    slot = lax.broadcasted_iota(jnp.int32, (slots, rows), 0) % MAIN
    named = (first_x + second_x) > 0.5
    pick_main = jnp.where(named & (rank_x == slot), 1.0, 0.0)
    pick_low = jnp.where(named & (rank_x == slot + MAIN) & (slot < REST), 1.0, 0.0)
    pick_high = jnp.where(named & (rank_x == slot + REST) & (slot >= REST), 1.0, 0.0)
    exp0 = jnp.exp(logits_ref[0:1, :])
    exp1 = jnp.exp(logits_ref[1:2, :])
    weight = (first_x * exp0 + second_x * exp1) / (exp0 + exp1)

    def split(table):
        turned = (table * weight).T
        top = turned.astype(BF16)
        return top, (turned - top.astype(F32)).astype(BF16)

    give_main, give_low, give_high = split(pick_main), split(pick_low), split(pick_high)
    pick_main, pick_low, pick_high = (t.astype(BF16) for t in (pick_main, pick_low, pick_high))

    take(rs_recv.at[pl.ds(1, depth - 1)], rs_sem)
    for dz in far:
        total = total + rs_recv[dz].astype(F32)
    own_resid = (tok_ref[...].astype(F32) + total).astype(BF16)
    resid_v[z] = own_resid

    ins = [(-j % depth, j + 1) for j in range(depth // 2)]
    pair_of = {dz: j for j, pair in enumerate(ins) for dz in pair}
    for dz in far:
        send(resid_v.at[z], resid_v.at[z], send_sem.at[2], ag_sem.at[pair_of[dz]], along(dz))
    two = 2 * LANES
    for j, (da, db) in enumerate(ins):
        if j:
            take(rs_recv.at[pl.ds(0, 2)], ag_sem.at[j])
        else:
            take(rs_recv.at[0], ag_sem.at[j])
        block_a, block_b = resid_v[down_z(da)], resid_v[down_z(db)]
        main = dot(pick_main, jnp.concatenate([block_a, block_b], axis=1)).astype(BF16)
        rest = (dot(pick_low, block_a) + dot(pick_high, block_b)).astype(BF16)
        disp_send[j, :, :, 0:two] = main.reshape(groups, MAIN, two)
        disp_send[j, :, :, two:] = rest.reshape(groups, MAIN, LANES)
        x_recv[core, j, 0] = disp_send[j, 0]
        for o in reversed(NEAR[1:]):
            src, dst = disp_send.at[j, o], x_recv.at[core, j, o]
            send(src, dst, send_sem.at[3], disp_sem.at[j], plane(o, 1))
    for j in range(len(ins)):
        take(x_recv.at[core, j, pl.ds(1, groups - 1)], disp_sem.at[j])
        block = x_recv.at[core, j]
        send(block, block, send_sem.at[4], relay_sem.at[j], partner)

    main_rows = groups * MAIN
    tile_row = lax.broadcasted_iota(jnp.int32, (groups // 2, MAIN, LANES), 1)
    upper = tile_row < REST
    squares = None
    for j, (da, db) in enumerate(ins):
        take(x_recv.at[other, j], relay_sem.at[j])
        if j == 0:
            take(wg_v, w_sem.at[0])
            take(wu_v, w_sem.at[1])
        mains, rests, gates, ups = [], [], [], []
        for p in range(2):
            got = x_recv[p, j].astype(F32)
            rest = got[:, :, two:].reshape(groups // 2, 2, MAIN, LANES)
            a, b = rest[:, 0], rest[:, 1]
            rest_a = jnp.where(upper, a, pltpu.roll(b, REST, 1)).reshape(-1, LANES)
            rest_b = jnp.where(upper, pltpu.roll(a, REST, 1), b).reshape(-1, LANES)
            for at, (dz, rest_d) in enumerate(((da, rest_a), (db, rest_b))):
                cols = pl.ds(pl.multiple_of((2 * down_z(dz) + p) * LANES, LANES), LANES)
                main = got[:, :, at * LANES : (at + 1) * LANES].reshape(main_rows, LANES)
                mains.append((main, gain_ref[:, cols]))
                rests.append((rest_d, gain_ref[:, cols]))
                gates.append(wg_v[:, cols])
                ups.append(wu_v[:, cols])
        parts = []
        for pieces in (mains, rests):
            squared = sum(jnp.sum(piece * piece, axis=1, keepdims=True) for piece, _ in pieces)
            scaled = jnp.concatenate([(piece * g).astype(BF16) for piece, g in pieces], axis=1)
            parts.append((squared, scaled))
        squared = jnp.concatenate([parts[0][0], parts[1][0]], axis=0)
        scaled = jnp.concatenate([parts[0][1], parts[1][1]], axis=0)
        gate = dot(scaled, jnp.concatenate(gates, axis=1), ((1,), (1,)))
        up = dot(scaled, jnp.concatenate(ups, axis=1), ((1,), (1,)))
        if j:
            squares = squares + squared
            gate = gate + gate_v[...]
            up = up + up_v[...]
        else:
            squares = squared
        if j < len(ins) - 1:
            gate_v[...] = gate
            up_v[...] = up
    scale = lax.rsqrt(squares * (1.0 / (2 * depth * LANES)) + RMS_EPS)
    gate = gate * scale
    hidden = (gate * jax.nn.sigmoid(gate) * (up * scale)).astype(BF16)

    take(wd_v, w_sem.at[2])
    outs = [(depth // 2 + j, depth // 2 - 1 - j) for j in range(depth // 2)]
    for j, pair in enumerate(outs):
        blocks = [up_z(dz) for dz in pair]
        y_send[j] = dot(hidden, wide(wd_v, other, blocks)).astype(BF16)
        send(y_send.at[j], y_recv.at[j], send_sem.at[5], y_sem.at[j], partner)
    for j, pair in enumerate(outs):
        blocks = [up_z(dz) for dz in pair]
        summed = dot(hidden, wide(wd_v, core, blocks))
        take(y_recv.at[j], y_sem.at[j])
        summed = summed + y_recv[j].astype(F32)
        ret_send[j, :, :, 0:two] = summed[:main_rows].astype(BF16).reshape(groups, MAIN, two)
        rest = summed[main_rows:].reshape(groups // 2, MAIN, two)
        rest_a, rest_b = rest[:, :, :LANES], rest[:, :, LANES:]
        even = jnp.where(upper, rest_a, pltpu.roll(rest_b, REST, 1)).astype(BF16)
        odd = jnp.where(upper, pltpu.roll(rest_a, REST, 1), rest_b).astype(BF16)
        for p in range(groups // 2):
            ret_send[j, 2 * p, :, two:] = even[p]
            ret_send[j, 2 * p + 1, :, two:] = odd[p]
        ret_recv[j, 0] = ret_send[j, 0]
        for o in reversed(NEAR[1:]):
            src, dst = ret_send.at[j, o], ret_recv.at[j, o]
            send(src, dst, send_sem.at[6], ret_sem.at[j], plane(o, -1))

    def give(tables, data):
        return dot(tables[0], data) + dot(tables[1], data)

    for j, (da, db) in enumerate(outs):
        take(ret_recv.at[j, pl.ds(1, groups - 1)], ret_sem.at[j])
        back = ret_recv[j]
        main = give(give_main, back[:, :, :two].reshape(slots, two))
        rest = back[:, :, two:].reshape(slots, LANES)
        for dz, moe in (
            (da, main[:, :LANES] + give(give_low, rest)),
            (db, main[:, LANES:] + give(give_high, rest)),
        ):
            if dz:
                moe_send[dz] = moe.astype(BF16)
                send(moe_send.at[dz], moe_recv.at[dz], send_sem.at[7], moe_sem, along(dz))
            else:
                total = own_resid.astype(F32) + moe
    take(moe_recv.at[pl.ds(1, depth - 1)], moe_sem)
    for dz in far:
        total = total + moe_recv[dz].astype(F32)
    out_ref[...] = total.astype(BF16)

    seven = pl.ds(1, depth - 1)
    take(pair_send, send_sem.at[0])
    take(rs_send.at[seven], send_sem.at[1])
    take(rs_send.at[seven], send_sem.at[2])
    take(disp_send.at[:, pl.ds(1, groups - 1)], send_sem.at[3])
    take(x_recv.at[core], send_sem.at[4])
    take(y_send, send_sem.at[5])
    take(ret_send.at[:, pl.ds(1, groups - 1)], send_sem.at[6])
    take(moe_send.at[seven], send_sem.at[7])


def local(
    tokens,
    state,
    routes,
    route_logits,
    mix_gain,
    w_recept,
    w_key,
    w_value,
    w_decay,
    w_rate,
    decay_base,
    rate_base,
    key_gain,
    group_gain,
    w_output,
    ffn_gain,
    w_gate,
    w_up,
    w_down,
):
    seqs, width = tokens.shape
    hidden = w_gate.shape[2]
    vmem = pl.BlockSpec(memory_space=pltpu.VMEM)
    anywhere = pl.BlockSpec(memory_space=pl.ANY)
    dma = pltpu.SemaphoreType.DMA

    def row(vector):
        return vector.reshape(1, -1)

    mixed, new_state = pl.pallas_call(
        mixer_kernel,
        out_shape=(
            jax.ShapeDtypeStruct((seqs, LANES), BF16),
            jax.ShapeDtypeStruct(state.shape, F32),
        ),
        in_specs=[anywhere] * 12,
        out_specs=(anywhere, anywhere),
        scratch_shapes=[
            pltpu.VMEM((seqs, LANES), BF16),
            pltpu.VMEM((seqs, width), BF16),
            pltpu.VMEM((1, width), F32),
            pltpu.VMEM((4, 1, LANES), F32),
            pltpu.VMEM((width, 5 * LANES), BF16),
            pltpu.VMEM(state.shape, F32),
            pltpu.VMEM(state.shape, F32),
            pltpu.VMEM((6, seqs, LANES), F32),
            pltpu.VMEM((2, seqs, LANES), F32),
            dma(()),
            dma(()),
            dma(()),
            dma(()),
            dma((CHUNKS,)),
            dma(()),
        ],
        compiler_params=pltpu.CompilerParams(vmem_limit_bytes=GRANT),
        name="mixer",
    )(
        tokens,
        state,
        row(mix_gain),
        w_recept,
        w_key,
        w_value,
        w_decay,
        w_rate,
        row(decay_base),
        row(rate_base),
        row(key_gain),
        row(group_gain),
    )

    depth = lax.axis_size("tp") // 2
    groups = SIDE * SIDE
    pairs = depth // 2
    message = (pairs, groups, MAIN, 3 * LANES)
    all_rows = groups * (MAIN + REST)
    block = (depth, seqs, LANES)
    output = pl.pallas_call(
        expert_kernel,
        out_shape=jax.ShapeDtypeStruct((seqs, LANES), BF16),
        in_specs=[anywhere] * 9,
        out_specs=vmem,
        scratch_shapes=[
            pltpu.VMEM((seqs, LANES), BF16),
            pltpu.VMEM((seqs, LANES), BF16),
            pltpu.VMEM(routes.shape[::-1], jnp.int32),
            pltpu.VMEM(routes.shape[::-1], F32),
            pltpu.VMEM((1, width), F32),
            pltpu.VMEM((2, depth, LANES, LANES), BF16),
            pltpu.VMEM((hidden, width), BF16),
            pltpu.VMEM((hidden, width), BF16),
            pltpu.VMEM((2, depth, hidden, LANES), BF16),
            pltpu.VMEM(block, BF16),
            pltpu.VMEM(block, BF16),
            pltpu.VMEM(block, F32),
            pltpu.VMEM(block, BF16),
            pltpu.VMEM(block, BF16),
            pltpu.VMEM(block, BF16),
            pltpu.VMEM(message, BF16),
            pltpu.VMEM((2,) + message, BF16),
            pltpu.VMEM((all_rows, hidden), F32),
            pltpu.VMEM((all_rows, hidden), F32),
            pltpu.VMEM((pairs, all_rows, 2 * LANES), BF16),
            pltpu.VMEM((pairs, all_rows, 2 * LANES), BF16),
            pltpu.VMEM(message, BF16),
            pltpu.VMEM(message, BF16),
            pltpu.VMEM(block, BF16),
            pltpu.VMEM(block, BF16),
            dma((6,)),
            dma((3,)),
            dma((8,)),
            dma(()),
            dma(()),
            dma((pairs,)),
            dma((pairs,)),
            dma((pairs,)),
            dma((pairs,)),
            dma((pairs,)),
            dma(()),
        ],
        compiler_params=pltpu.CompilerParams(
            collective_id=0, has_side_effects=True, vmem_limit_bytes=GRANT
        ),
        name="experts",
    )(
        mixed,
        tokens,
        routes.T,
        route_logits.T,
        row(ffn_gain),
        w_output,
        jnp.swapaxes(w_gate, 1, 2)[0],
        jnp.swapaxes(w_up, 1, 2)[0],
        w_down[0],
    )
    return (output, new_state)


def solution(mesh):
    return jax.shard_map(
        local,
        mesh=mesh,
        in_specs=(
            P("ep", None),
            P("ep", "tp", None, None),
            P("ep", None),
            P("ep", None),
            P(),
            P(None, "tp"),
            P(None, "tp"),
            P(None, "tp"),
            P(None, "tp"),
            P(None, "tp"),
            P("tp"),
            P("tp"),
            P("tp"),
            P("tp"),
            P("tp", None),
            P(),
            P("ep", None, "tp"),
            P("ep", None, "tp"),
            P("ep", "tp", None),
        ),
        out_specs=(P("ep", "tp"), P("ep", "tp", None, None)),
        check_vma=False,
    )
```

time: 66.4 us -> 52.2 us (0.79)
  local copies, waits for them, and re-layouts: 12.3 us -> 1.32 us
  Pallas kernels: 52.9 us -> 49.9 us
    unnamed x39 -> x1, local copies, waits for them, and re-layouts: 12.3 us -> 1.32 us
    pallas_call x1, Pallas kernels: 46.9 us -> 43.9 us  [local(): pl.pallas_call(expert_kernel, out_shape=jax.ShapeDtypeStruct((seqs, LANES...]
where the time goes in v2:
time: 52.2 us; the launch traced here: 51.9 us
  Pallas kernels  49.9 us (96%)
  local copies, waits for them, and re-layouts  1.32 us (3%)
  between operations  0.65 us (1%)
    pallas_call x1, Pallas kernels, local(): pl.pallas_call(expert_kernel, out_shape=jax.ShapeDtypeStruct((seqs, LANES...  43.9 us
    pallas_call x1, Pallas kernels, local(): pl.pallas_call(mixer_kernel, out_shape=(jax.ShapeDtypeStruct((seqs, LANES...  6.01 us
    unnamed x1, local copies, waits for them, and re-layouts  1.32 us

profile of v2, /device:TPU:1, one launch (start us, length us, event | category | flops | bytes accessed | tf_op | source)
XLA Modules:
  0.0 51.9 jit_solution(3368609156875220738)
XLA Ops:
  0.6 6.0 %mixer.1 = (bf16[64,128]{1,0:T(8,128)(2,1)}, f32[64,2,64,64]{3,2,1,0:T(8,128)}) custom-call(bf16[64,2048]{1,0:T(8,128)(2,1)} %tok_hbm.3, f32[64,2,64,64]{3,2,1,0:T(8,128)} %st_hbm.1, f32[1,2048]{1,0:T(1,128)} %bitcast.18, bf16[2048,128]{1,0:T(8,128)(2,1)} %w_recept.1, bf16[2048,128]{1,0:T(8,128)(2,1)} %w_key.1, bf16[2048,128]{1,0:T(8,128)(2,1)} %w_value.1, ...), custom_call_target="tpu_custom_call" | custom-call | tf_op jit(solution)/shard_map/mixer/pallas_call | solution.py:489
  6.7 43.9 %experts.1 = bf16[64,128]{1,0:T(8,128)(2,1)} custom-call(bf16[64,128]{1,0:T(8,128)(2,1)} %get-tuple-element.4.mixed_hbm, bf16[64,2048]{1,0:T(8,128)(2,1)} %tok_hbm.3, s32[2,64]{1,0:T(2,128)} %bitcast.20, f32[2,64]{1,0:T(2,128)} %bitcast.21, f32[1,2048]{1,0:T(1,128)} %bitcast.19, bf16[128,2048]{1,0:T(8,128)(2,1)} %wo_hbm.1, bf16[448,2048]{1,0:T(8,128)(2,1)} %bitcast.15, ...), custom_call_target="tpu_custom_call" | custom-call | tf_op jit(solution)/shard_map/experts/pallas_call | solution.py:537
  50.6 1.3 %copy.22 = bf16[64,128]{1,0:T(8,128)(2,1)} copy(bf16[64,128]{1,0:T(8,128)(2,1)} %experts.1) | data formatting | bytes 32768

commit v3 on v2

--- a/solution.py
+++ b/solution.py
@@ -17,6 +17,7 @@
 SIDE = 4
 CHUNKS = 4
 PAIR = 8
+PIECES = 8
 MAIN = 8
 REST = 4
 GRANT = 67043328
@@ -28,135 +29,138 @@
     return lax.dot_general(a, b, (contract, ((), ())), preferred_element_type=F32)
 
 
-def mixer_kernel(
+def mixer(refs):
+    (tok_hbm, st_hbm, gain_hbm, w_hbms, vec_hbms, ns_hbm) = refs[:6]
+    (tok_v, gain_v, vec_v, w_v, st_v, ns_v, rows_v, read_v) = refs[6:14]
+    (tok_sem, gain_sem, vec_sem, w_sem, st_sem, ns_sem) = refs[14:]
+    seqs = tok_v.shape[0]
+    per = seqs // CHUNKS
+    tok_copy = pltpu.make_async_copy(tok_hbm, tok_v, tok_sem)
+    tok_copy.start()
+    gain_copy = pltpu.make_async_copy(gain_hbm, gain_v, gain_sem)
+    gain_copy.start()
+    for j, w_hbm in enumerate(w_hbms):
+        pltpu.make_async_copy(w_hbm, w_v.at[:, pl.ds(j * LANES, LANES)], w_sem).start()
+    for j, vec_hbm in enumerate(vec_hbms):
+        pltpu.make_async_copy(vec_hbm, vec_v.at[j], vec_sem).start()
+
+    def st_copy(i):
+        part = pl.ds(i * per, per)
+        return pltpu.make_async_copy(st_hbm.at[part], st_v.at[part], st_sem.at[i])
+
+    def ns_copy(i):
+        part = pl.ds(i * per, per)
+        return pltpu.make_async_copy(ns_v.at[part], ns_hbm.at[part], ns_sem)
+
+    lane = lax.broadcasted_iota(jnp.int32, (seqs, LANES), 1)
+
+    def per_head(values):
+        first = jnp.sum(jnp.where(lane < HALF, values, 0.0), axis=1, keepdims=True)
+        second = jnp.sum(jnp.where(lane < HALF, 0.0, values), axis=1, keepdims=True)
+        return jnp.where(lane < HALF, first, second)
+
+    wide = 2 * LANES
+    block_r = lax.broadcasted_iota(jnp.int32, (wide, wide), 0) // HALF
+    block_c = lax.broadcasted_iota(jnp.int32, (wide, wide), 1) // HALF
+    diag = (
+        lax.broadcasted_iota(jnp.int32, (HALF, LANES), 0)
+        == lax.broadcasted_iota(jnp.int32, (HALF, LANES), 1) % HALF
+    )[None]
+
+    def old_state(part):
+        return jnp.concatenate([st_v[part, 0], st_v[part, 1]], axis=-1)
+
+    def row_of(j, part):
+        return rows_v[j, part][:, None, :]
+
+    def flat(values):
+        return values.astype(BF16).reshape(PAIR * HALF, LANES)
+
+    def head_sums(left, right):
+        ones = (block_r == block_c).astype(BF16)
+        both = dot(jnp.concatenate([flat(left), flat(right)], axis=1), ones)
+        return (
+            both[:, :LANES].reshape(PAIR, HALF, LANES),
+            both[:, LANES:].reshape(PAIR, HALF, LANES),
+        )
+
+    def mixed_rows(fetch_rest):
+        tok_copy.wait()
+        for i in range(CHUNKS):
+            st_copy(i).start()
+        fetch_rest()
+        values = tok_v[...].astype(F32)
+        scale = lax.rsqrt(jnp.mean(values * values, axis=1, keepdims=True) + RMS_EPS)
+        gain_copy.wait()
+        normed = (values * scale * gain_v[...]).astype(BF16)
+        pltpu.make_async_copy(w_v, w_v, w_sem).wait()
+        pltpu.make_async_copy(vec_v, vec_v, vec_sem).wait()
+        decay_base, rate_base, key_gain, group_gain = (vec_v[j] for j in range(4))
+        projected = dot(normed, w_v[...]).astype(BF16).astype(F32)
+        recept, key, value, decay_in, rate_in = (
+            projected[:, j * LANES : (j + 1) * LANES] for j in range(5)
+        )
+        decay = jnp.exp(-(0.6065306597126334 * jax.nn.sigmoid(decay_in + decay_base)))
+        rate = jax.nn.sigmoid(rate_in + rate_base)
+        scaled = key * key_gain
+        unit = scaled * lax.rsqrt(per_head(scaled * scaled) + UNIT_EPS)
+        rows_v[0] = unit
+        rows_v[1] = decay
+        rows_v[2] = unit * rate
+        rows_v[3] = key
+        rows_v[4] = decay * recept
+        rows_v[5] = value
+
+        def look(i, carry):
+            st_copy(i).wait()
+            for p in range(per // PAIR):
+                part = pl.ds(i * per + p * PAIR, PAIR)
+                old = old_state(part)
+                removed, seen = head_sums(old * row_of(0, part), old * row_of(4, part))
+                read_v[0, part, :] = jnp.sum(jnp.where(diag, removed, 0.0), axis=1)
+                read_v[1, part, :] = jnp.sum(jnp.where(diag, seen, 0.0), axis=1)
+            return carry
+
+        lax.fori_loop(0, CHUNKS, look, 0)
+        taken = read_v[0] * per_head(unit * rate * recept)
+        readout = read_v[1] - taken + value * per_head(key * recept)
+        centred = readout - per_head(readout) * (1.0 / HALF)
+        spread = per_head(centred * centred) * (1.0 / HALF)
+        return (centred * lax.rsqrt(spread + GROUP_EPS) * group_gain).astype(BF16)
+
+    def update():
+        def chunk(i, carry):
+            for p in range(per // PAIR):
+                part = pl.ds(i * per + p * PAIR, PAIR)
+                old = old_state(part)
+                spread = jnp.where(diag, row_of(5, part), 0.0)
+                removed, value = head_sums(old * row_of(0, part), spread)
+                new = old * row_of(1, part) - removed * row_of(2, part) + value * row_of(3, part)
+                ns_v[part] = new
+            ns_copy(i).start()
+            return carry
+
+        lax.fori_loop(0, CHUNKS, chunk, 0)
+
+    def finish():
+        pltpu.make_async_copy(ns_v, ns_hbm, ns_sem).wait()
+
+    return mixed_rows, update, finish
+
+
+def layer_kernel(
     tok_hbm,
     st_hbm,
-    gain_hbm,
-    w_recept,
-    w_key,
-    w_value,
-    w_decay,
-    w_rate,
+    mix_gain_hbm,
+    wr_hbm,
+    wk_hbm,
+    wv_hbm,
+    wdec_hbm,
+    wrate_hbm,
     decay_hbm,
     rate_hbm,
     key_hbm,
     group_hbm,
-    mixed_hbm,
-    ns_hbm,
-    mixed_ref,
-    tok_v,
-    mix_gain,
-    vec_v,
-    w_v,
-    st_v,
-    ns_v,
-    rows_v,
-    read_v,
-    tok_sem,
-    gain_sem,
-    vec_sem,
-    w_sem,
-    st_sem,
-    ns_sem,
-):
-    seqs = tok_v.shape[0]
-    per = seqs // CHUNKS
-    tok_copy = pltpu.make_async_copy(tok_hbm, tok_v, tok_sem)
-    tok_copy.start()
-    gain_copy = pltpu.make_async_copy(gain_hbm, mix_gain, gain_sem)
-    gain_copy.start()
-    for j, w_hbm in enumerate((w_recept, w_key, w_value, w_decay, w_rate)):
-        pltpu.make_async_copy(w_hbm, w_v.at[:, pl.ds(j * LANES, LANES)], w_sem).start()
-    for j, vec_hbm in enumerate((decay_hbm, rate_hbm, key_hbm, group_hbm)):
-        pltpu.make_async_copy(vec_hbm, vec_v.at[j], vec_sem).start()
-
-    def st_copy(i):
-        part = pl.ds(i * per, per)
-        return pltpu.make_async_copy(st_hbm.at[part], st_v.at[part], st_sem.at[i])
-
-    def ns_copy(i):
-        part = pl.ds(i * per, per)
-        return pltpu.make_async_copy(ns_v.at[part], ns_hbm.at[part], ns_sem)
-
-    lane = lax.broadcasted_iota(jnp.int32, (seqs, LANES), 1)
-
-    def per_head(values):
-        first = jnp.sum(jnp.where(lane < HALF, values, 0.0), axis=1, keepdims=True)
-        second = jnp.sum(jnp.where(lane < HALF, 0.0, values), axis=1, keepdims=True)
-        return jnp.where(lane < HALF, first, second)
-
-    tok_copy.wait()
-    for i in range(CHUNKS):
-        st_copy(i).start()
-    values = tok_v[...].astype(F32)
-    scale = lax.rsqrt(jnp.mean(values * values, axis=1, keepdims=True) + RMS_EPS)
-    gain_copy.wait()
-    normed = (values * scale * mix_gain[...]).astype(BF16)
-    pltpu.make_async_copy(w_v, w_v, w_sem).wait()
-    pltpu.make_async_copy(vec_v, vec_v, vec_sem).wait()
-    decay_base, rate_base, key_gain, group_gain = (vec_v[j] for j in range(4))
-    projected = dot(normed, w_v[...]).astype(BF16).astype(F32)
-    recept, key, value, decay_in, rate_in = (
-        projected[:, j * LANES : (j + 1) * LANES] for j in range(5)
-    )
-    decay = jnp.exp(-(0.6065306597126334 * jax.nn.sigmoid(decay_in + decay_base)))
-    rate = jax.nn.sigmoid(rate_in + rate_base)
-    scaled = key * key_gain
-    unit = scaled * lax.rsqrt(per_head(scaled * scaled) + UNIT_EPS)
-    rows_v[0] = unit
-    rows_v[1] = decay
-    rows_v[2] = unit * rate
-    rows_v[3] = key
-    rows_v[4] = decay * recept
-    rows_v[5] = value
-
-    wide = 2 * LANES
-    block_r = lax.broadcasted_iota(jnp.int32, (wide, wide), 0) // HALF
-    block_c = lax.broadcasted_iota(jnp.int32, (wide, wide), 1) // HALF
-    ones2 = (block_r == block_c).astype(BF16)
-    ones1 = ones2[:LANES, :LANES]
-    diag = (
-        lax.broadcasted_iota(jnp.int32, (HALF, LANES), 0)
-        == lax.broadcasted_iota(jnp.int32, (HALF, LANES), 1) % HALF
-    )[None]
-
-    def chunk(i, carry):
-        st_copy(i).wait()
-        for p in range(per // PAIR):
-            part = pl.ds(i * per + p * PAIR, PAIR)
-            old = jnp.concatenate([st_v[part, 0], st_v[part, 1]], axis=-1)
-            unit_c, decay_c, take_c, key_c, seen_c, value_c = (
-                rows_v[j, part][:, None, :] for j in range(6)
-            )
-            probe = (old * unit_c).astype(BF16).reshape(PAIR * HALF, LANES)
-            spread = jnp.where(diag, value_c, 0.0).astype(BF16).reshape(PAIR * HALF, LANES)
-            both = dot(jnp.concatenate([probe, spread], axis=1), ones2)
-            seen = dot((old * seen_c).astype(BF16).reshape(PAIR * HALF, LANES), ones1)
-            removed = both[:, :LANES].reshape(PAIR, HALF, LANES)
-            value_b = both[:, LANES:].reshape(PAIR, HALF, LANES)
-            new = old * decay_c - removed * take_c + value_b * key_c
-            ns_v[part, 0] = new[..., :HALF]
-            ns_v[part, 1] = new[..., HALF:]
-            read_v[0, part, :] = jnp.sum(jnp.where(diag, removed, 0.0), axis=1)
-            seen = jnp.where(diag, seen.reshape(PAIR, HALF, LANES), 0.0)
-            read_v[1, part, :] = jnp.sum(seen, axis=1)
-        ns_copy(i).start()
-        return carry
-
-    lax.fori_loop(0, CHUNKS, chunk, 0)
-    readout = read_v[1] - read_v[0] * per_head(unit * rate * recept) + value * per_head(key * recept)
-    centred = readout - per_head(readout) * (1.0 / HALF)
-    spread = per_head(centred * centred) * (1.0 / HALF)
-    mixed_ref[...] = (centred * lax.rsqrt(spread + GROUP_EPS) * group_gain).astype(BF16)
-    mixed_copy = pltpu.make_async_copy(mixed_ref, mixed_hbm, tok_sem)
-    mixed_copy.start()
-    pltpu.make_async_copy(ns_v, ns_hbm, ns_sem).wait()
-    mixed_copy.wait()
-
-
-def expert_kernel(
-    mixed_hbm,
-    tok_hbm,
     routes_hbm,
     logits_hbm,
     gain_hbm,
@@ -165,7 +169,15 @@
     wu_hbm,
     wd_hbm,
     out_ref,
-    mixed_ref,
+    ns_hbm,
+    mtok_v,
+    mgain_v,
+    vec_v,
+    w_v,
+    st_v,
+    ns_v,
+    rows_v,
+    read_v,
     tok_ref,
     routes_ref,
     logits_ref,
@@ -190,6 +202,12 @@
     ret_recv,
     moe_send,
     moe_recv,
+    mtok_sem,
+    mgain_sem,
+    vec_sem,
+    mw_sem,
+    st_sem,
+    ns_sem,
     in_sem,
     w_sem,
     send_sem,
@@ -244,29 +262,47 @@
     def fetch(src, dst, sem):
         pltpu.make_async_copy(src, dst, sem).start()
 
+    mixed_rows, update, finish = mixer(
+        (
+            tok_hbm,
+            st_hbm,
+            mix_gain_hbm,
+            (wr_hbm, wk_hbm, wv_hbm, wdec_hbm, wrate_hbm),
+            (decay_hbm, rate_hbm, key_hbm, group_hbm),
+            ns_hbm,
+            mtok_v,
+            mgain_v,
+            vec_v,
+            w_v,
+            st_v,
+            ns_v,
+            rows_v,
+            read_v,
+            mtok_sem,
+            mgain_sem,
+            vec_sem,
+            mw_sem,
+            st_sem,
+            ns_sem,
+        )
+    )
     barrier = pltpu.get_barrier_semaphore()
     peers = [partner] + [along(dz) for dz in range(1, depth)]
     peers += [plane(o, 1) for o in range(1, groups)]
     for peer in peers:
         pl.semaphore_signal(barrier, inc=1, device_id=peer, device_id_type=MESH)
 
-    fetch(mixed_hbm, mixed_ref, in_sem.at[0])
-    for j in range(2 * depth):
-        fetch(wo_hbm.at[:, pl.ds(j * LANES, LANES)], wo_v.at[j % 2, j // 2], in_sem.at[1])
-    own_cols = pl.ds(pl.multiple_of(tp * LANES, LANES), LANES)
-    fetch(routes_hbm, routes_ref, in_sem.at[2])
-    fetch(logits_hbm, logits_ref, in_sem.at[3])
-    fetch(tok_hbm.at[:, own_cols], tok_ref, in_sem.at[4])
-    fetch(gain_hbm, gain_ref, in_sem.at[5])
-
-    take(mixed_ref, in_sem.at[0])
-    take(wo_v, in_sem.at[1])
-    fetch(wg_hbm, wg_v, w_sem.at[0])
-    fetch(wu_hbm, wu_v, w_sem.at[1])
-    for j in range(2 * depth):
-        fetch(wd_hbm.at[:, pl.ds(j * LANES, LANES)], wd_v.at[j % 2, j // 2], w_sem.at[2])
-
-    mixed = mixed_ref[...]
+    def fetch_rest():
+        for j in range(2 * depth):
+            fetch(wo_hbm.at[:, pl.ds(j * LANES, LANES)], wo_v.at[j % 2, j // 2], in_sem.at[0])
+        own_cols = pl.ds(pl.multiple_of(tp * LANES, LANES), LANES)
+        fetch(routes_hbm, routes_ref, in_sem.at[1])
+        fetch(logits_hbm, logits_ref, in_sem.at[2])
+        fetch(tok_hbm.at[:, own_cols], tok_ref, in_sem.at[3])
+        fetch(gain_hbm, gain_ref, in_sem.at[4])
+
+    mixed = mixed_rows(fetch_rest)
+    take(wo_v, in_sem.at[0])
 
     def wide(ref, side, blocks):
         return jnp.concatenate([ref[side, k] for k in blocks], axis=1)
@@ -276,6 +312,10 @@
         pair_send[k] = theirs[:, k * LANES : (k + 1) * LANES]
     pl.semaphore_wait(barrier, len(peers))
     send(pair_send, pair_recv, send_sem.at[0], pair_sem, partner)
+    fetch(wg_hbm, wg_v, w_sem.at[0])
+    fetch(wu_hbm, wu_v, w_sem.at[1])
+    for j in range(2 * depth):
+        fetch(wd_hbm.at[:, pl.ds(j * LANES, LANES)], wd_v.at[j % 2, j // 2], w_sem.at[2])
     mine = dot(mixed, wide(wo_v, core, range(depth)))
     for k in range(depth):
         own_v[k] = mine[:, k * LANES : (k + 1) * LANES]
@@ -289,7 +329,7 @@
     total = own_v[z] + pair_recv[z].astype(F32)
 
     for j, ref in enumerate((routes_ref, logits_ref, tok_ref, gain_ref)):
-        take(ref, in_sem.at[2 + j])
+        take(ref, in_sem.at[1 + j])
     row16 = lax.broadcasted_iota(jnp.int32, (groups, rows), 0)
     expert = (((y + (row16 >> 2)) & 3) << 2) | ((x + (row16 & 3)) & 3)
     first = (routes_ref[0:1, :] == expert).astype(BF16)
@@ -324,6 +364,7 @@
     give_main, give_low, give_high = split(pick_main), split(pick_low), split(pick_high)
     pick_main, pick_low, pick_high = (t.astype(BF16) for t in (pick_main, pick_low, pick_high))
 
+    update()
     take(rs_recv.at[pl.ds(1, depth - 1)], rs_sem)
     for dz in far:
         total = total + rs_recv[dz].astype(F32)
@@ -332,7 +373,7 @@
 
     ins = [(-j % depth, j + 1) for j in range(depth // 2)]
     pair_of = {dz: j for j, pair in enumerate(ins) for dz in pair}
-    for dz in far:
+    for dz in reversed(far):
         send(resid_v.at[z], resid_v.at[z], send_sem.at[2], ag_sem.at[pair_of[dz]], along(dz))
     two = 2 * LANES
     for j, (da, db) in enumerate(ins):
@@ -445,6 +486,7 @@
         total = total + moe_recv[dz].astype(F32)
     out_ref[...] = total.astype(BF16)
 
+    finish()
     seven = pl.ds(1, depth - 1)
     take(pair_send, send_sem.at[0])
     take(rs_send.at[seven], send_sem.at[1])
@@ -454,6 +496,34 @@
     take(y_send, send_sem.at[5])
     take(ret_send.at[:, pl.ds(1, groups - 1)], send_sem.at[6])
     take(moe_send.at[seven], send_sem.at[7])
+
+
+def unpack_kernel(
+    out_hbm, packed_hbm, copy_hbm, state_hbm, out_v, packed_v, state_v, out_sem, in_sem, st_sem
+):
+    per = packed_v.shape[0] // PIECES
+
+    def piece(i):
+        part = pl.ds(i * per, per)
+        return pltpu.make_async_copy(packed_hbm.at[part], packed_v.at[part], in_sem.at[i])
+
+    for i in range(PIECES):
+        piece(i).start()
+    take_out = pltpu.make_async_copy(out_hbm, out_v, out_sem.at[0])
+    take_out.start()
+    give_out = pltpu.make_async_copy(out_v, copy_hbm, out_sem.at[1])
+    for i in range(PIECES):
+        part = pl.ds(i * per, per)
+        piece(i).wait()
+        both = packed_v[part]
+        state_v[part, 0] = both[..., :HALF]
+        state_v[part, 1] = both[..., HALF:]
+        pltpu.make_async_copy(state_v.at[part], state_hbm.at[part], st_sem).start()
+        if i == 0:
+            take_out.wait()
+            give_out.start()
+    give_out.wait()
+    pltpu.make_async_copy(state_v, state_hbm, st_sem).wait()
 
 
 def local(
@@ -486,61 +556,30 @@
     def row(vector):
         return vector.reshape(1, -1)
 
-    mixed, new_state = pl.pallas_call(
-        mixer_kernel,
-        out_shape=(
-            jax.ShapeDtypeStruct((seqs, LANES), BF16),
-            jax.ShapeDtypeStruct(state.shape, F32),
-        ),
-        in_specs=[anywhere] * 12,
-        out_specs=(anywhere, anywhere),
-        scratch_shapes=[
-            pltpu.VMEM((seqs, LANES), BF16),
-            pltpu.VMEM((seqs, width), BF16),
-            pltpu.VMEM((1, width), F32),
-            pltpu.VMEM((4, 1, LANES), F32),
-            pltpu.VMEM((width, 5 * LANES), BF16),
-            pltpu.VMEM(state.shape, F32),
-            pltpu.VMEM(state.shape, F32),
-            pltpu.VMEM((6, seqs, LANES), F32),
-            pltpu.VMEM((2, seqs, LANES), F32),
-            dma(()),
-            dma(()),
-            dma(()),
-            dma(()),
-            dma((CHUNKS,)),
-            dma(()),
-        ],
-        compiler_params=pltpu.CompilerParams(vmem_limit_bytes=GRANT),
-        name="mixer",
-    )(
-        tokens,
-        state,
-        row(mix_gain),
-        w_recept,
-        w_key,
-        w_value,
-        w_decay,
-        w_rate,
-        row(decay_base),
-        row(rate_base),
-        row(key_gain),
-        row(group_gain),
-    )
-
     depth = lax.axis_size("tp") // 2
     groups = SIDE * SIDE
     pairs = depth // 2
     message = (pairs, groups, MAIN, 3 * LANES)
     all_rows = groups * (MAIN + REST)
     block = (depth, seqs, LANES)
-    output = pl.pallas_call(
-        expert_kernel,
-        out_shape=jax.ShapeDtypeStruct((seqs, LANES), BF16),
-        in_specs=[anywhere] * 9,
-        out_specs=vmem,
+    packed = (seqs, state.shape[2], LANES)
+    output, new_state = pl.pallas_call(
+        layer_kernel,
+        out_shape=(
+            jax.ShapeDtypeStruct((seqs, LANES), BF16),
+            jax.ShapeDtypeStruct(packed, F32),
+        ),
+        in_specs=[anywhere] * 19,
+        out_specs=(vmem, anywhere),
         scratch_shapes=[
-            pltpu.VMEM((seqs, LANES), BF16),
+            pltpu.VMEM((seqs, width), BF16),
+            pltpu.VMEM((1, width), F32),
+            pltpu.VMEM((4, 1, LANES), F32),
+            pltpu.VMEM((width, 5 * LANES), BF16),
+            pltpu.VMEM(state.shape, F32),
+            pltpu.VMEM(packed, F32),
+            pltpu.VMEM((6, seqs, LANES), F32),
+            pltpu.VMEM((2, seqs, LANES), F32),
             pltpu.VMEM((seqs, LANES), BF16),
             pltpu.VMEM(routes.shape[::-1], jnp.int32),
             pltpu.VMEM(routes.shape[::-1], F32),
@@ -565,7 +604,13 @@
             pltpu.VMEM(message, BF16),
             pltpu.VMEM(block, BF16),
             pltpu.VMEM(block, BF16),
-            dma((6,)),
+            dma(()),
+            dma(()),
+            dma(()),
+            dma(()),
+            dma((CHUNKS,)),
+            dma(()),
+            dma((5,)),
             dma((3,)),
             dma((8,)),
             dma(()),
@@ -580,10 +625,20 @@
         compiler_params=pltpu.CompilerParams(
             collective_id=0, has_side_effects=True, vmem_limit_bytes=GRANT
         ),
-        name="experts",
+        name="layer",
     )(
-        mixed,
         tokens,
+        state,
+        row(mix_gain),
+        w_recept,
+        w_key,
+        w_value,
+        w_decay,
+        w_rate,
+        row(decay_base),
+        row(rate_base),
+        row(key_gain),
+        row(group_gain),
         routes.T,
         route_logits.T,
         row(ffn_gain),
@@ -592,7 +647,25 @@
         jnp.swapaxes(w_up, 1, 2)[0],
         w_down[0],
     )
-    return (output, new_state)
+    return pl.pallas_call(
+        unpack_kernel,
+        out_shape=(
+            jax.ShapeDtypeStruct((seqs, LANES), BF16),
+            jax.ShapeDtypeStruct(state.shape, F32),
+        ),
+        in_specs=[anywhere] * 2,
+        out_specs=(anywhere, anywhere),
+        scratch_shapes=[
+            pltpu.VMEM((seqs, LANES), BF16),
+            pltpu.VMEM(packed, F32),
+            pltpu.VMEM(state.shape, F32),
+            dma((2,)),
+            dma((PIECES,)),
+            dma(()),
+        ],
+        compiler_params=pltpu.CompilerParams(vmem_limit_bytes=GRANT),
+        name="unpack",
+    )(output, new_state)
 
 
 def solution(mesh):

time: 52.2 us -> 48.9 us (0.937)
  Pallas kernels: 49.9 us -> 48.1 us
  local copies, waits for them, and re-layouts: 1.32 us -> 0 us
    pallas_call x2, Pallas kernels: 49.9 us -> 48.1 us  [the longest x1 44.7 us: local(): pl.pallas_call(layer_kernel, out_shape=(jax.ShapeDtypeStruct((seqs, LANES...]
    unnamed x1 -> x0, local copies, waits for them, and re-layouts: 1.32 us -> none
where the time goes in v3:
time: 48.9 us; the launch traced here: 48.8 us
  Pallas kernels  48.1 us (98%)
  between operations  0.65 us (1%)
    pallas_call x1, Pallas kernels, local(): pl.pallas_call(layer_kernel, out_shape=(jax.ShapeDtypeStruct((seqs, LANES...  44.7 us
    pallas_call x1, Pallas kernels, local(): pl.pallas_call(unpack_kernel, out_shape=(jax.ShapeDtypeStruct((seqs, LANE...  3.4 us

profile of v3, /device:TPU:1, one launch (start us, length us, event | category | flops | bytes accessed | tf_op | source)
XLA Modules:
  0.0 48.8 jit_solution(2561289930487948531)
XLA Ops:
  0.6 44.7 %layer.1 = (bf16[64,128]{1,0:T(8,128)(2,1)}, f32[64,64,128]{2,1,0:T(8,128)}) custom-call(bf16[64,2048]{1,0:T(8,128)(2,1)} %tok_hbm.1, f32[64,2,64,64]{3,2,1,0:T(8,128)} %st_hbm.1, f32[1,2048]{1,0:T(1,128)} %bitcast.18, bf16[2048,128]{1,0:T(8,128)(2,1)} %wr_hbm.1, bf16[2048,128]{1,0:T(8,128)(2,1)} %wk_hbm.1, bf16[2048,128]{1,0:T(8,128)(2,1)} %wv_hbm.1, ...), custom_call_target="tpu_custom_call" | custom-call | tf_op jit(solution)/shard_map/layer/pallas_call | solution.py:566
  45.4 3.4 %unpack.1 = (bf16[64,128]{1,0:T(8,128)(2,1)}, f32[64,2,64,64]{3,2,1,0:T(8,128)}) custom-call(bf16[64,128]{1,0:T(8,128)(2,1)} %get-tuple-element.4.out_hbm, f32[64,64,128]{2,1,0:T(8,128)} %get-tuple-element.5.packed_hbm), custom_call_target="tpu_custom_call" | custom-call | tf_op jit(solution)/shard_map/unpack/pallas_call | solution.py:650

commit v4 on v3

--- a/solution.py
+++ b/solution.py
@@ -39,10 +39,12 @@
     tok_copy.start()
     gain_copy = pltpu.make_async_copy(gain_hbm, gain_v, gain_sem)
     gain_copy.start()
-    for j, w_hbm in enumerate(w_hbms):
-        pltpu.make_async_copy(w_hbm, w_v.at[:, pl.ds(j * LANES, LANES)], w_sem).start()
-    for j, vec_hbm in enumerate(vec_hbms):
-        pltpu.make_async_copy(vec_hbm, vec_v.at[j], vec_sem).start()
+
+    def fetch_weights():
+        for j, w_hbm in enumerate(w_hbms):
+            pltpu.make_async_copy(w_hbm, w_v.at[:, pl.ds(j * LANES, LANES)], w_sem).start()
+        for j, vec_hbm in enumerate(vec_hbms):
+            pltpu.make_async_copy(vec_hbm, vec_v.at[j], vec_sem).start()
 
     def st_copy(i):
         part = pl.ds(i * per, per)
@@ -145,7 +147,7 @@
     def finish():
         pltpu.make_async_copy(ns_v, ns_hbm, ns_sem).wait()
 
-    return mixed_rows, update, finish
+    return fetch_weights, mixed_rows, update, finish
 
 
 def layer_kernel(
@@ -198,6 +200,7 @@
     up_v,
     y_send,
     y_recv,
+    y_own,
     ret_send,
     ret_recv,
     moe_send,
@@ -262,7 +265,7 @@
     def fetch(src, dst, sem):
         pltpu.make_async_copy(src, dst, sem).start()
 
-    mixed_rows, update, finish = mixer(
+    fetch_weights, mixed_rows, update, finish = mixer(
         (
             tok_hbm,
             st_hbm,
@@ -291,6 +294,7 @@
     peers += [plane(o, 1) for o in range(1, groups)]
     for peer in peers:
         pl.semaphore_signal(barrier, inc=1, device_id=peer, device_id_type=MESH)
+    fetch_weights()
 
     def fetch_rest():
         for j in range(2 * depth):
@@ -359,9 +363,10 @@
     def split(table):
         turned = (table * weight).T
         top = turned.astype(BF16)
-        return top, (turned - top.astype(F32)).astype(BF16)
-
-    give_main, give_low, give_high = split(pick_main), split(pick_low), split(pick_high)
+        return jnp.concatenate([top, (turned - top.astype(F32)).astype(BF16)], axis=1)
+
+    give_main = split(pick_main)
+    give_rest = jnp.concatenate([split(pick_low), split(pick_high)], axis=0)
     pick_main, pick_low, pick_high = (t.astype(BF16) for t in (pick_main, pick_low, pick_high))
 
     update()
@@ -442,15 +447,17 @@
 
     take(wd_v, w_sem.at[2])
     outs = [(depth // 2 + j, depth // 2 - 1 - j) for j in range(depth // 2)]
-    for j, pair in enumerate(outs):
-        blocks = [up_z(dz) for dz in pair]
-        y_send[j] = dot(hidden, wide(wd_v, other, blocks)).astype(BF16)
+    out_blocks = [up_z(dz) for pair in outs for dz in pair]
+    theirs = dot(hidden, wide(wd_v, other, out_blocks)).astype(BF16)
+    for j in range(len(outs)):
+        y_send[j] = theirs[:, j * two : (j + 1) * two]
         send(y_send.at[j], y_recv.at[j], send_sem.at[5], y_sem.at[j], partner)
-    for j, pair in enumerate(outs):
-        blocks = [up_z(dz) for dz in pair]
-        summed = dot(hidden, wide(wd_v, core, blocks))
+    mine = dot(hidden, wide(wd_v, core, out_blocks))
+    for j in range(len(outs)):
+        y_own[j] = mine[:, j * two : (j + 1) * two]
+    for j in range(len(outs)):
         take(y_recv.at[j], y_sem.at[j])
-        summed = summed + y_recv[j].astype(F32)
+        summed = y_own[j] + y_recv[j].astype(F32)
         ret_send[j, :, :, 0:two] = summed[:main_rows].astype(BF16).reshape(groups, MAIN, two)
         rest = summed[main_rows:].reshape(groups // 2, MAIN, two)
         rest_a, rest_b = rest[:, :, :LANES], rest[:, :, LANES:]
@@ -465,16 +472,16 @@
             send(src, dst, send_sem.at[6], ret_sem.at[j], plane(o, -1))
 
     def give(tables, data):
-        return dot(tables[0], data) + dot(tables[1], data)
+        return dot(tables, jnp.concatenate([data, data], axis=0))
 
     for j, (da, db) in enumerate(outs):
         take(ret_recv.at[j, pl.ds(1, groups - 1)], ret_sem.at[j])
         back = ret_recv[j]
         main = give(give_main, back[:, :, :two].reshape(slots, two))
-        rest = back[:, :, two:].reshape(slots, LANES)
+        rest = give(give_rest, back[:, :, two:].reshape(slots, LANES))
         for dz, moe in (
-            (da, main[:, :LANES] + give(give_low, rest)),
-            (db, main[:, LANES:] + give(give_high, rest)),
+            (da, main[:, :LANES] + rest[:rows]),
+            (db, main[:, LANES:] + rest[rows:]),
         ):
             if dz:
                 moe_send[dz] = moe.astype(BF16)
@@ -507,10 +514,10 @@
         part = pl.ds(i * per, per)
         return pltpu.make_async_copy(packed_hbm.at[part], packed_v.at[part], in_sem.at[i])
 
+    take_out = pltpu.make_async_copy(out_hbm, out_v, out_sem.at[0])
+    take_out.start()
     for i in range(PIECES):
         piece(i).start()
-    take_out = pltpu.make_async_copy(out_hbm, out_v, out_sem.at[0])
-    take_out.start()
     give_out = pltpu.make_async_copy(out_v, copy_hbm, out_sem.at[1])
     for i in range(PIECES):
         part = pl.ds(i * per, per)
@@ -519,7 +526,7 @@
         state_v[part, 0] = both[..., :HALF]
         state_v[part, 1] = both[..., HALF:]
         pltpu.make_async_copy(state_v.at[part], state_hbm.at[part], st_sem).start()
-        if i == 0:
+        if i == 1:
             take_out.wait()
             give_out.start()
     give_out.wait()
@@ -600,6 +607,7 @@
             pltpu.VMEM((all_rows, hidden), F32),
             pltpu.VMEM((pairs, all_rows, 2 * LANES), BF16),
             pltpu.VMEM((pairs, all_rows, 2 * LANES), BF16),
+            pltpu.VMEM((pairs, all_rows, 2 * LANES), F32),
             pltpu.VMEM(message, BF16),
             pltpu.VMEM(message, BF16),
             pltpu.VMEM(block, BF16),

time: 48.9 us -> 47.9 us (0.980)
  Pallas kernels: 48.1 us -> 47.1 us
    pallas_call x1, Pallas kernels: 44.7 us -> 43.9 us  [local(): pl.pallas_call(layer_kernel, out_shape=(jax.ShapeDtypeStruct((seqs, LANES...]
where the time goes in v4:
time: 47.9 us; the launch traced here: 47.8 us
  Pallas kernels  47.1 us (98%)
  between operations  0.65 us (1%)
    pallas_call x1, Pallas kernels, local(): pl.pallas_call(layer_kernel, out_shape=(jax.ShapeDtypeStruct((seqs, LANES...  43.9 us
    pallas_call x1, Pallas kernels, local(): pl.pallas_call(unpack_kernel, out_shape=(jax.ShapeDtypeStruct((seqs, LANE...  3.18 us

profile of v4, /device:TPU:1, one launch (start us, length us, event | category | flops | bytes accessed | tf_op | source)
XLA Modules:
  0.0 47.8 jit_solution(972657892215672647)
XLA Ops:
  0.6 43.9 %layer.1 = (bf16[64,128]{1,0:T(8,128)(2,1)}, f32[64,64,128]{2,1,0:T(8,128)}) custom-call(bf16[64,2048]{1,0:T(8,128)(2,1)} %tok_hbm.1, f32[64,2,64,64]{3,2,1,0:T(8,128)} %st_hbm.1, f32[1,2048]{1,0:T(1,128)} %bitcast.18, bf16[2048,128]{1,0:T(8,128)(2,1)} %wr_hbm.1, bf16[2048,128]{1,0:T(8,128)(2,1)} %wk_hbm.1, bf16[2048,128]{1,0:T(8,128)(2,1)} %wv_hbm.1, ...), custom_call_target="tpu_custom_call" | custom-call | tf_op jit(solution)/shard_map/layer/pallas_call | solution.py:573
  44.6 3.2 %unpack.1 = (bf16[64,128]{1,0:T(8,128)(2,1)}, f32[64,2,64,64]{3,2,1,0:T(8,128)}) custom-call(bf16[64,128]{1,0:T(8,128)(2,1)} %get-tuple-element.4.out_hbm, f32[64,64,128]{2,1,0:T(8,128)} %get-tuple-element.5.packed_hbm), custom_call_target="tpu_custom_call" | custom-call | tf_op jit(solution)/shard_map/unpack/pallas_call | solution.py:658
